TPU v7x, 256 devices: a whole 4x4x8 slice. The times are simulated.
256 devices in a mesh: ep: 16 (over y, x), tp: 16 (over z, core).
Axes of the slice: x: 4, y: 4, z: 8, core: 2. Of those that a mesh axis runs over, the one named last changes fastest.
Arguments:
- hidden: bfloat16 [640, 4096], P('ep', 'tp'), may hold values from -6 to 6
- positions: int32 [640], P('ep'), may hold values from 0 to 16383
- ret_state: float32 [640, 16, 128, 128], P('ep', 'tp'), may hold values from -1.5 to 1.5
- query_weight: bfloat16 [4096, 2048], P('ep', 'tp'), may hold values from -0.09375 to 0.09375
- key_weight: bfloat16 [4096, 2048], P('ep', 'tp'), may hold values from -0.09375 to 0.09375
- value_weight: bfloat16 [4096, 2048], P('ep', 'tp'), may hold values from -0.09375 to 0.09375
- gate_weight: bfloat16 [4096, 2048], P('ep', 'tp'), may hold values from -0.09375 to 0.09375
- head_gain: float32 [2048], P('tp'), may hold values from 0.1 to 1.9
- out_weight: bfloat16 [2048, 4096], P(None, 'tp'), may hold values from -0.125 to 0.125
- mix_gain: float32 [4096], replicated, may hold values from 0.1 to 1.9
- ffn_gain: float32 [4096], replicated, may hold values from 0.1 to 1.9
- expert_gate: bfloat16 [32, 4096, 2048], P('ep', None, 'tp'), may hold values from -0.09375 to 0.09375
- expert_up: bfloat16 [32, 4096, 2048], P('ep', None, 'tp'), may hold values from -0.09375 to 0.09375
- expert_down: bfloat16 [32, 2048, 4096], P('ep', None, 'tp'), may hold values from -0.125 to 0.125
- route_ids: int32 [640, 2], P('ep'), may hold values from 0 to 31, as said below
- route_weight: float32 [640, 2], P('ep'), may hold values from 0.25 to 1
Outputs:
- updated: bfloat16 [640, 4096], P('ep', 'tp')
- next_state: float32 [640, 16, 128, 128], P('ep', 'tp')
Inputs may be any that keep to these rules, and one draw needn't show every extreme that they name: `route_ids`: each row names two different experts of one group, the group being the numbers g * 8 to g * 8 + 7; in the rows of one device (aligned blocks of 40 rows) no expert is named more than 4 times, and some expert is named exactly 4 times.
All inputs are finite; a program needn't handle non-finite values.
Results may differ from a plain program's by a relative error of at most 0.014.
Values may be sent and summed in bfloat16 or wider, within the bound.
A program may use at most 64 MiB of HBM per device.

v0:
```python
import jax
import jax.numpy as jnp
from jax import lax
from jax.sharding import PartitionSpec as P

D = 4096
HEADS = 16
HEAD = 128
GROUPS = 4
TOP = 2


epsilon = 1e-06
rope_base = 10000.0


def joined_along(blocks, dim):
    dims = list(blocks.shape[1:])
    dims[dim] *= blocks.shape[0]
    return jnp.moveaxis(blocks, 0, dim).reshape(dims)


def from_everyone(array, axis):
    size = lax.axis_size(axis)
    return lax.all_to_all(
        jnp.broadcast_to(array[None], (size, *array.shape)), axis, 0, 0, tiled=True
    )


def gathered_copies(array, axis, dim):
    return joined_along(from_everyone(array, axis), dim)


def split_up(array, dim, size):
    dims = array.shape
    blocks = array.reshape(*dims[:dim], size, dims[dim] // size, *dims[dim + 1 :])
    return jnp.moveaxis(blocks, dim, 0)


def summed_on_arrival(array, axis, dim):
    blocks = split_up(array, dim, lax.axis_size(axis))
    arrived = lax.all_to_all(blocks, axis, split_axis=0, concat_axis=0, tiled=True)
    return arrived.sum(axis=0)


def rms_scale(rows, gain):
    values = rows.astype(jnp.float32)
    factor = lax.rsqrt(jnp.mean(values * values, axis=-1, keepdims=True) + epsilon)
    return (values * factor * gain).astype(jnp.bfloat16)


def log_decay(head_ids):
    return jnp.log(1.0 - 2.0 ** (-5.0 - 5.0 * head_ids.astype(jnp.float32) / (HEADS - 1)))


def rotate(values, positions):
    width = values.shape[-1]
    inverse = 1.0 / rope_base ** (jnp.arange(0, width, 2, dtype=jnp.float32) / width)
    angle = positions.astype(jnp.float32)[:, None, None] * inverse[None, None, :]
    cosine = jnp.cos(angle)
    sine = jnp.sin(angle)
    first = values[..., : width // 2]
    second = values[..., width // 2 :]
    return jnp.concatenate(
        [first * cosine - second * sine, first * sine + second * cosine], axis=-1
    )


def retain(query, key_rows, value_rows, gate_rows, ret_state, positions, head_ids, head_gain):
    batch = query.shape[0]
    heads = head_ids.shape[0]

    def split(array):
        return array.astype(jnp.float32).reshape(batch, heads, HEAD)

    rotated_query = rotate(split(query), positions)
    rotated_key = rotate(split(key_rows), positions) * HEAD ** (-0.5)
    value_heads = split(value_rows)
    decay = jnp.exp(log_decay(head_ids))
    next_state = (
        decay[None, :, None, None] * ret_state
        + rotated_key[..., :, None] * value_heads[..., None, :]
    )
    read = jnp.einsum("bhd,bhde->bhe", rotated_query, next_state)
    centered = read - jnp.mean(read, axis=-1, keepdims=True)
    normal = centered * lax.rsqrt(jnp.mean(centered * centered, axis=-1, keepdims=True) + epsilon)
    mixed = (
        normal.reshape(batch, heads * HEAD) * head_gain * jax.nn.silu(gate_rows.astype(jnp.float32))
    )
    return (mixed.astype(jnp.bfloat16), next_state)


def per_device(
    hidden,
    positions,
    ret_state,
    query_weight,
    key_weight,
    value_weight,
    gate_weight,
    head_gain,
    out_weight,
    mix_gain,
    ffn_gain,
    expert_gate,
    expert_up,
    expert_down,
    route_ids,
    route_weight,
):
    own_rows = hidden.shape[0]
    full_rows = gathered_copies(hidden, "tp", 1)
    normed = rms_scale(full_rows, mix_gain)
    columns = lax.all_to_all(normed, "ep", split_axis=1, concat_axis=0, tiled=True)
    stacked = jnp.concatenate([query_weight, key_weight, value_weight, gate_weight], axis=1)
    width = query_weight.shape[1]
    joined = summed_on_arrival(
        jnp.dot(columns, stacked, preferred_element_type=jnp.float32), "ep", 0
    )
    sums = tuple((joined[:, number * width : (number + 1) * width] for number in range(4)))
    query, key_rows, value_rows, gate_rows = tuple((total.astype(jnp.bfloat16) for total in sums))
    heads_here = query_weight.shape[1] // HEAD
    head_ids = lax.axis_index("tp") * heads_here + jnp.arange(heads_here, dtype=jnp.int32)
    mixed, next_state = retain(
        query, key_rows, value_rows, gate_rows, ret_state, positions, head_ids, head_gain
    )
    projected = jnp.dot(
        gathered_copies(mixed, "tp", 1), out_weight, preferred_element_type=jnp.float32
    )
    after = (hidden.astype(jnp.float32) + projected).astype(jnp.bfloat16)
    local_experts = expert_gate.shape[0]
    peers = lax.axis_size("ep")
    experts = local_experts * peers
    group_size = experts // GROUPS
    capacity = 2 * ((own_rows // GROUPS + group_size - 1) // group_size)
    chosen = route_ids.reshape(-1)
    onehot = (chosen[:, None] == jnp.arange(experts, dtype=jnp.int32)[None, :]).astype(jnp.int32)
    ranks = jnp.sum((jnp.cumsum(onehot, axis=0) - 1) * onehot, axis=1)
    send_slot = chosen * capacity + ranks
    slot_count = experts * capacity
    placing = (jnp.arange(slot_count, dtype=jnp.int32)[:, None] == send_slot[None, :]).astype(
        jnp.float32
    )
    token_place = jnp.sum(placing.reshape(slot_count, own_rows, TOP), axis=2).astype(jnp.bfloat16)
    whole_rows = gathered_copies(after, "tp", 1)
    source = rms_scale(whole_rows, ffn_gain)
    packed = jnp.dot(token_place, source, preferred_element_type=jnp.float32).astype(jnp.bfloat16)
    arrived = lax.all_to_all(
        packed.reshape(peers, local_experts, capacity, source.shape[1]),
        "ep",
        split_axis=0,
        concat_axis=2,
        tiled=True,
    )
    arrived = arrived.reshape(local_experts, peers * capacity, D)
    gate = jnp.einsum("emd,edf->emf", arrived, expert_gate, preferred_element_type=jnp.float32)
    lifted = jnp.einsum("emd,edf->emf", arrived, expert_up, preferred_element_type=jnp.float32)
    activated = (jax.nn.silu(gate) * lifted).astype(jnp.bfloat16)
    out_width = expert_down.shape[2]
    result = jnp.einsum(
        "emf,efd->emd",
        gathered_copies(activated, "tp", 2),
        expert_down,
        preferred_element_type=jnp.float32,
    ).astype(jnp.bfloat16)
    back = lax.all_to_all(
        result.reshape(local_experts, peers, capacity, out_width),
        "ep",
        split_axis=1,
        concat_axis=1,
        tiled=True,
    )
    returned_rows = back.reshape(local_experts * peers * capacity, out_width)
    source_row = (
        chosen % local_experts * (peers * capacity) + chosen // local_experts * capacity + ranks
    )
    values = returned_rows[source_row].astype(jnp.float32).reshape(own_rows, TOP, out_width)
    weighted = jnp.sum(values * route_weight[:, :, None], axis=1)
    updated = (after.astype(jnp.float32) + weighted).astype(jnp.bfloat16)
    return (updated, next_state)


def solution(mesh):
    return jax.shard_map(
        per_device,
        mesh=mesh,
        in_specs=(
            P("ep", "tp"),
            P("ep"),
            P("ep", "tp", None, None),
            P("ep", "tp"),
            P("ep", "tp"),
            P("ep", "tp"),
            P("ep", "tp"),
            P("tp"),
            P(None, "tp"),
            P(),
            P(),
            P("ep", None, "tp"),
            P("ep", None, "tp"),
            P("ep", None, "tp"),
            P("ep", None),
            P("ep", None),
        ),
        out_specs=(P("ep", "tp"), P("ep", "tp", None, None)),
        check_vma=False,
    )
```

profile of v0, /device:TPU:1, one launch (start us, length us, event | category | flops | bytes accessed | tf_op | source)
XLA Modules:
  0.0 167.4 jit_solution(9162365699423734746)
XLA Ops:
  0.6 0.0 copy-start
  0.6 0.0 copy-start.4
  0.7 1.6 broadcast_in_dim.8
  2.3 10.0 %all-to-all-start = ((bf16[16,40,256]{2,1,0:T(8,128)(2,1)}), bf16[16,40,256]{2,1,0:T(8,128)(2,1)S(1)}, u32[]{:S(2)}, u32[]{:S(2)}) async-start(bf16[16,40,256]{2,1,0:T(8,128)(2,1)} %broadcast_in_dim.8), calls=%async_computation | async-start | bytes 655360 | tf_op jit(solution)/shard_map/all_to_all | solution.py:25
  12.3 0.7 mul.230
  13.0 12.2 %all-to-all-done = bf16[16,40,256]{2,1,0:T(8,128)(2,1)S(1)} async-done(((bf16[16,40,256]{2,1,0:T(8,128)(2,1)}), bf16[16,40,256]{2,1,0:T(8,128)(2,1)S(1)}, u32[]{:S(2)}, u32[]{:S(2)}) %all-to-all-start) | async-done | bytes 327712 | tf_op jit(solution)/shard_map/all_to_all | solution.py:25
  25.3 0.2 fusion.4
  25.4 0.2 fusion.10
  25.6 0.0 copy-start.12
  25.6 16.0 %all_to_all.58 = bf16[40,16,256]{2,0,1:T(8,128)(2,1)S(1)} all-to-all(bf16[40,16,256]{2,0,1:T(8,128)(2,1)S(1)} %fusion.10), channel_id=1, replica_groups=mesh['ep'=16,'tp'=16] {'ep'}, dimensions={1} | all-to-all | bytes 655360 | tf_op jit(solution)/shard_map/all_to_all | solution.py:114
  41.6 1.4 fusion.11
  43.0 3.7 %all-to-all-start.2 = ((f32[16,40,512]{2,1,0:T(8,128)}), f32[16,40,512]{2,1,0:T(8,128)S(1)}, u32[]{:S(2)}, u32[]{:S(2)}) async-start(f32[16,40,512]{2,1,0:T(8,128)} %fusion.11), calls=%async_computation.2 | async-start | bytes 2621440 | tf_op jit(solution)/shard_map/all_to_all | solution.py:42
  46.7 0.0 copy-start.11
  46.7 0.0 copy-start.9
  46.8 0.0 copy-start.3
  46.9 18.7 %all-to-all-done.2 = f32[16,40,512]{2,1,0:T(8,128)S(1)} async-done(((f32[16,40,512]{2,1,0:T(8,128)}), f32[16,40,512]{2,1,0:T(8,128)S(1)}, u32[]{:S(2)}, u32[]{:S(2)}) %all-to-all-start.2) | async-done | bytes 1310752 | tf_op jit(solution)/shard_map/all_to_all | solution.py:42
  65.7 0.1 reduce_sum.77
  65.8 0.0 copy-start.2
  65.8 0.2 fusion.39
  66.0 0.1 maximum_multiply_fusion
  66.0 0.1 pad_maximum_fusion
  66.1 2.6 %fusion.52 = f32[40,1,128]{2,1,0:T(1,128)S(1)} fusion(f32[40,128,1]{1,2,0:T(1,128)S(1)} %bitcast.82, f32[40,128]{1,0:T(8,128)S(1)} %get-tuple-element.3, f32[40,128]{1,0:T(8,128)S(1)} %maximum_multiply_fusion, f32[40,1,128,128]{3,2,1,0:T(8,128)} %param.18, f32[]{:T(128)S(6)} %exp.14), kind=kOutput, calls=%fused_computation.92 | convolution fusion | flops 3276800 | bytes 2703364 | tf_op jit(solution)/shard_map/bhd,bhde->bhe/dot_general | solution.py:84
  68.7 0.1 reduce_sum.78
  68.8 0.2 multiply_reduce_fusion.1
  69.0 0.1 fusion.42
  69.1 0.7 broadcast_in_dim.9
  69.8 6.2 %all-to-all-start.3 = ((bf16[16,40,128]{2,1,0:T(8,128)(2,1)}), bf16[16,40,128]{2,1,0:T(8,128)(2,1)S(1)}, u32[]{:S(2)}, u32[]{:S(2)}) async-start(bf16[16,40,128]{2,1,0:T(8,128)(2,1)} %broadcast_in_dim.9), calls=%async_computation.3 | async-start | bytes 327680 | tf_op jit(solution)/shard_map/all_to_all | solution.py:25
  76.0 0.0 copy-start.8
  76.1 0.1 copy.54
  76.1 0.1 eq.32
  76.3 9.4 %all-to-all-done.3 = bf16[16,40,128]{2,1,0:T(8,128)(2,1)S(1)} async-done(((bf16[16,40,128]{2,1,0:T(8,128)(2,1)}), bf16[16,40,128]{2,1,0:T(8,128)(2,1)S(1)}, u32[]{:S(2)}, u32[]{:S(2)}) %all-to-all-start.3) | async-done | bytes 163872 | tf_op jit(solution)/shard_map/all_to_all | solution.py:25
  85.7 0.3 fusion.3
  86.0 0.7 broadcast_in_dim.10
  86.7 3.4 %all-to-all-start.4 = ((bf16[16,40,256]{2,1,0:T(8,128)(2,1)}), bf16[16,40,256]{2,1,0:T(8,128)(2,1)S(1)}, u32[]{:S(2)}, u32[]{:S(2)}) async-start(bf16[16,40,256]{2,1,0:T(8,128)(2,1)} %broadcast_in_dim.10), calls=%async_computation.4 | async-start | bytes 655360 | tf_op jit(solution)/shard_map/all_to_all | solution.py:25
  90.2 0.1 fusion.23
  90.2 0.1 reduce_window_sum.11
  90.4 0.2 select_reduce_fusion
  90.5 0.1 reduce_sum.81
  90.7 0.1 copy.55
  90.7 0.1 convert_reduce_fusion
  90.8 12.2 %all-to-all-done.4 = bf16[16,40,256]{2,1,0:T(8,128)(2,1)S(1)} async-done(((bf16[16,40,256]{2,1,0:T(8,128)(2,1)}), bf16[16,40,256]{2,1,0:T(8,128)(2,1)S(1)}, u32[]{:S(2)}, u32[]{:S(2)}) %all-to-all-start.4) | async-done | bytes 327712 | tf_op jit(solution)/shard_map/all_to_all | solution.py:25
  103.1 0.2 fusion.7
  103.4 0.5 convolution_convert_fusion
  103.9 1.2 reshape.402
  105.1 22.0 %all_to_all.59 = bf16[16,2,4,4096]{3,2,1,0:T(4,128)(2,1)S(1)} all-to-all(bf16[16,2,4,4096]{3,2,1,0:T(4,128)(2,1)} %reshape.402), channel_id=1, replica_groups=mesh['ep'=16,'tp'=16] {'ep'}, dimensions={0} | all-to-all | bytes 2097152 | tf_op jit(solution)/shard_map/all_to_all | solution.py:148
  127.1 1.4 copy.57
  128.5 1.3 reshape.403
  129.9 0.0 copy-start.1
  129.9 2.2 %fusion.55 = f32[2,64,128]{2,1,0:T(8,128)S(1)} fusion(bf16[2,64,4096]{2,1,0:T(8,128)(2,1)S(1)} %reshape.403, bf16[2,4096,128]{2,1,0:T(8,128)(2,1)} %param.27), kind=kOutput, calls=%fused_computation.94 | convolution fusion | flops 134217728 | bytes 3211264 | tf_op jit(solution)/shard_map/emd,edf->emf/dot_general | solution.py:156
  132.2 0.0 copy-start.10
  132.2 0.5 fusion.2
  132.7 0.9 broadcast_in_dim.11
  133.6 3.7 %all-to-all-start.6 = ((bf16[16,2,64,128]{3,2,1,0:T(8,128)(2,1)}), bf16[16,2,64,128]{3,2,1,0:T(8,128)(2,1)S(1)}, u32[]{:S(2)}, u32[]{:S(2)}) async-start(bf16[16,2,64,128]{3,2,1,0:T(8,128)(2,1)} %broadcast_in_dim.11), calls=%async_computation.6 | async-start | bytes 1048576 | tf_op jit(solution)/shard_map/all_to_all | solution.py:25
  137.3 0.1 reshape.407
  137.4 0.1 copy.62
  137.6 17.1 %all-to-all-done.6 = bf16[16,2,64,128]{3,2,1,0:T(8,128)(2,1)S(1)} async-done(((bf16[16,2,64,128]{3,2,1,0:T(8,128)(2,1)}), bf16[16,2,64,128]{3,2,1,0:T(8,128)(2,1)S(1)}, u32[]{:S(2)}, u32[]{:S(2)}) %all-to-all-start.6) | async-done | bytes 524320 | tf_op jit(solution)/shard_map/all_to_all | solution.py:25
  154.6 0.5 convolution_convert_fusion.1
  155.1 0.6 copy.59
  155.8 3.5 %all-to-all-start.7 = ((bf16[2,16,4,256]{3,2,0,1:T(4,128)(2,1)}), bf16[2,16,4,256]{3,2,0,1:T(4,128)(2,1)S(1)}, u32[]{:S(2)}, u32[]{:S(2)}) async-start(bf16[2,16,4,256]{3,2,0,1:T(4,128)(2,1)} %copy.59), calls=%async_computation.7 | async-start | bytes 131072 | tf_op jit(solution)/shard_map/all_to_all | solution.py:166
  159.3 3.3 %multiply_add_fusion = f32[40,1,128,128]{3,2,1,0:T(8,128)} fusion(f32[40,1,128,128]{3,2,1,0:T(8,128)} %param.18, f32[]{:T(128)S(6)} %exp.14, f32[40,128]{1,0:T(8,128)S(1)} %get-tuple-element.3, f32[40,128]{1,0:T(8,128)S(1)} %maximum_multiply_fusion), kind=kLoop, calls=%fused_computation.4 | loop fusion | flops 1966080 | bytes 5283844 | tf_op jit(solution)/shard_map/add | solution.py:81
  162.6 3.2 %all-to-all-done.7 = bf16[2,16,4,256]{3,2,0,1:T(4,128)(2,1)S(1)} async-done(((bf16[2,16,4,256]{3,2,0,1:T(4,128)(2,1)}), bf16[2,16,4,256]{3,2,0,1:T(4,128)(2,1)S(1)}, u32[]{:S(2)}, u32[]{:S(2)}) %all-to-all-start.7) | async-done | bytes 65568 | tf_op jit(solution)/shard_map/all_to_all | solution.py:166
  165.8 0.7 gather_fusion
  166.6 0.2 multiply_reduce_fusion
  166.8 0.6 add_convert_fusion
  (32 shorter events, 0.3 us)
Async XLA Ops:
  0.6 154.0 %copy-start = (bf16[2,2048,256]{2,1,0:T(8,128)(2,1)S(1)}, bf16[2,2048,256]{2,1,0:T(8,128)(2,1)}, u32[]{:S(2)}) copy-start(bf16[2,2048,256]{2,1,0:T(8,128)(2,1)} %param.29) | copy-start | bytes 6291460
  0.6 41.0 %copy-start.4 = (bf16[256,128]{1,0:T(8,128)(2,1)S(1)}, bf16[256,128]{1,0:T(8,128)(2,1)}, u32[]{:S(2)}) copy-start(bf16[256,128]{1,0:T(8,128)(2,1)} %param.22) | copy-start | bytes 196612
  0.7 41.0 %copy-start.5 = (bf16[256,128]{1,0:T(8,128)(2,1)S(1)}, bf16[256,128]{1,0:T(8,128)(2,1)}, u32[]{:S(2)}) copy-start(bf16[256,128]{1,0:T(8,128)(2,1)} %param.21) | copy-start | bytes 196612
  0.7 40.9 %copy-start.6 = (bf16[256,128]{1,0:T(8,128)(2,1)S(1)}, bf16[256,128]{1,0:T(8,128)(2,1)}, u32[]{:S(2)}) copy-start(bf16[256,128]{1,0:T(8,128)(2,1)} %param.20) | copy-start | bytes 196612
  0.7 40.9 %copy-start.7 = (bf16[256,128]{1,0:T(8,128)(2,1)S(1)}, bf16[256,128]{1,0:T(8,128)(2,1)}, u32[]{:S(2)}) copy-start(bf16[256,128]{1,0:T(8,128)(2,1)} %param.19) | copy-start | bytes 196612
  2.3 22.9 %all-to-all-start = ((bf16[16,40,256]{2,1,0:T(8,128)(2,1)}), bf16[16,40,256]{2,1,0:T(8,128)(2,1)S(1)}, u32[]{:S(2)}, u32[]{:S(2)}) async-start(bf16[16,40,256]{2,1,0:T(8,128)(2,1)} %broadcast_in_dim.8), calls=%async_computation | async-start | bytes 655360 | tf_op jit(solution)/shard_map/all_to_all | solution.py:25
  25.6 21.3 %copy-start.12 = (s32[40]{0:T(128)S(1)}, s32[40]{0:T(128)}, u32[]{:S(2)}) copy-start(s32[40]{0:T(128)} %param.17) | copy-start | bytes 484
  43.0 22.7 %all-to-all-start.2 = ((f32[16,40,512]{2,1,0:T(8,128)}), f32[16,40,512]{2,1,0:T(8,128)S(1)}, u32[]{:S(2)}, u32[]{:S(2)}) async-start(f32[16,40,512]{2,1,0:T(8,128)} %fusion.11), calls=%async_computation.2 | async-start | bytes 2621440 | tf_op jit(solution)/shard_map/all_to_all | solution.py:42
  46.7 22.3 %copy-start.11 = (f32[128]{0:T(128)S(1)}, f32[128]{0:T(128)}, u32[]{:S(2)}) copy-start(f32[128]{0:T(128)} %param.23) | copy-start | bytes 1540
  46.7 29.3 %copy-start.9 = (s32[40,2]{0,1:T(2,128)S(1)}, s32[40,2]{0,1:T(2,128)}, u32[]{:S(2)}) copy-start(s32[40,2]{0,1:T(2,128)} %param.30) | copy-start | bytes 964
  46.8 38.9 %copy-start.3 = (bf16[40,256]{1,0:T(8,128)(2,1)S(1)}, bf16[40,256]{1,0:T(8,128)(2,1)}, u32[]{:S(2)}) copy-start(bf16[40,256]{1,0:T(8,128)(2,1)} %param.16) | copy-start | bytes 61444
  65.8 19.9 %copy-start.2 = (bf16[2048,256]{1,0:T(8,128)(2,1)S(1)}, bf16[2048,256]{1,0:T(8,128)(2,1)}, u32[]{:S(2)}) copy-start(bf16[2048,256]{1,0:T(8,128)(2,1)} %param.24) | copy-start | bytes 3145732
  69.8 15.8 %all-to-all-start.3 = ((bf16[16,40,128]{2,1,0:T(8,128)(2,1)}), bf16[16,40,128]{2,1,0:T(8,128)(2,1)S(1)}, u32[]{:S(2)}, u32[]{:S(2)}) async-start(bf16[16,40,128]{2,1,0:T(8,128)(2,1)} %broadcast_in_dim.9), calls=%async_computation.3 | async-start | bytes 327680 | tf_op jit(solution)/shard_map/all_to_all | solution.py:25
  76.0 27.3 %copy-start.8 = (f32[4096]{0:T(1024)S(1)}, f32[4096]{0:T(1024)}, u32[]{:S(2)}) copy-start(f32[4096]{0:T(1024)} %param.26) | copy-start | bytes 49156
  86.7 16.3 %all-to-all-start.4 = ((bf16[16,40,256]{2,1,0:T(8,128)(2,1)}), bf16[16,40,256]{2,1,0:T(8,128)(2,1)S(1)}, u32[]{:S(2)}, u32[]{:S(2)}) async-start(bf16[16,40,256]{2,1,0:T(8,128)(2,1)} %broadcast_in_dim.10), calls=%async_computation.4 | async-start | bytes 655360 | tf_op jit(solution)/shard_map/all_to_all | solution.py:25
  129.9 2.3 %copy-start.1 = (bf16[2,4096,128]{2,1,0:T(8,128)(2,1)S(1)}, bf16[2,4096,128]{2,1,0:T(8,128)(2,1)}, u32[]{:S(2)}) copy-start(bf16[2,4096,128]{2,1,0:T(8,128)(2,1)} %param.28) | copy-start | bytes 6291460
  132.2 5.3 %copy-start.10 = (f32[40,2]{0,1:T(2,128)S(1)}, f32[40,2]{0,1:T(2,128)}, u32[]{:S(2)}) copy-start(f32[40,2]{0,1:T(2,128)} %param.31) | copy-start | bytes 964
  133.6 21.1 %all-to-all-start.6 = ((bf16[16,2,64,128]{3,2,1,0:T(8,128)(2,1)}), bf16[16,2,64,128]{3,2,1,0:T(8,128)(2,1)S(1)}, u32[]{:S(2)}, u32[]{:S(2)}) async-start(bf16[16,2,64,128]{3,2,1,0:T(8,128)(2,1)} %broadcast_in_dim.11), calls=%async_computation.6 | async-start | bytes 1048576 | tf_op jit(solution)/shard_map/all_to_all | solution.py:25
  155.8 9.9 %all-to-all-start.7 = ((bf16[2,16,4,256]{3,2,0,1:T(4,128)(2,1)}), bf16[2,16,4,256]{3,2,0,1:T(4,128)(2,1)S(1)}, u32[]{:S(2)}, u32[]{:S(2)}) async-start(bf16[2,16,4,256]{3,2,0,1:T(4,128)(2,1)} %copy.59), calls=%async_computation.7 | async-start | bytes 131072 | tf_op jit(solution)/shard_map/all_to_all | solution.py:166
where the time goes:
time: 168 us; the launch traced here: 167 us
  waiting for transfers between devices  72.8 us (43%)
  blocking collectives  38 us (23%)
  starting transfers between devices  30.6 us (18%)
  local copies, waits for them, and re-layouts  10.9 us (6%)
  matrix products  7.99 us (5%)
  other arithmetic  5.93 us (4%)
    all_to_all x4, waiting for transfers between devices, from_everyone(): lax.all_to_all(jnp.broadcast_to(array[None], (size, *array.shape)), axis,...  50.9 us
    all_to_all x4, starting transfers between devices, from_everyone(): lax.all_to_all(jnp.broadcast_to(array[None], (size, *array.shape)), axis,...  23.4 us
    all_to_all x1, blocking collectives, per_device(): lax.all_to_all(packed.reshape(peers, local_experts, capacity, source.shap...  22 us
    all_to_all x1, waiting for transfers between devices, summed_on_arrival(): lax.all_to_all(blocks, axis, split_axis=0, concat_axis=0, tiled=True)  18.7 us
    all_to_all x1, blocking collectives, per_device(): lax.all_to_all(normed, 'ep', split_axis=1, concat_axis=0, tiled=True)  16 us
    broadcast_in_dim x4, local copies, waits for them, and re-layouts, from_everyone(): jnp.broadcast_to(array[None], (size, *array.shape))  3.98 us
    all_to_all x1, starting transfers between devices, summed_on_arrival(): lax.all_to_all(blocks, axis, split_axis=0, concat_axis=0, tiled=True)  3.7 us
    all_to_all x1, starting transfers between devices, per_device(): lax.all_to_all(result.reshape(local_experts, peers, capacity, out_width),...  3.48 us
  transfers between devices with their start and end apart: 6, of which 6 were waited for; matrix products, arithmetic and copies ran while one was open for 3% of the time, Pallas kernels for 0%

commit v1 on v0

v1 whole, which is shorter than its diff:
```python
import functools

import jax
import jax.numpy as jnp
import numpy as np
from jax import lax
from jax.experimental import pallas as pl
from jax.experimental.pallas import tpu as pltpu
from jax.sharding import PartitionSpec as P

MESH = pl.DeviceIdType.MESH
F32 = jnp.float32
BF16 = jnp.bfloat16
D = 4096
RD = 2048
HEADS = 16
HEAD = 128
ROWS = 40
COLS = 256
NEP = 16
NTP = 16
NZ = 8
SLOTS = 128
EPS = 1e-06


def constants():
    table = np.zeros((24, 128), np.float64)
    heads = np.arange(HEADS, dtype=np.float64)
    table[:HEADS] = (1.0 - 2.0 ** (-5.0 - 5.0 * heads / (HEADS - 1)))[:, None]
    inverse = 10000.0 ** (-np.arange(0, HEAD, 2, dtype=np.float64) / HEAD)
    table[HEADS] = np.concatenate([inverse, inverse])
    return table.astype(np.float32)


def ring_offset(i):
    half = i // 2 + 1
    return half + (i % 2) * (NZ - 2 * half)


def body(
    hidden,
    positions,
    ret_state,
    query_weight,
    key_weight,
    value_weight,
    gate_weight,
    head_gain,
    out_weight,
    mix_gain,
    ffn_gain,
    expert_gate,
    expert_up,
    expert_down,
    route_ids,
    route_weight,
    table,
    updated,
    next_state,
    v_hidden,
    v_pos,
    v_state,
    v_qkvg,
    v_head_gain,
    v_out,
    v_mix_gain,
    v_ffn_gain,
    v_gu,
    v_down,
    v_ids,
    v_weight,
    v_table,
    agbuf,
    xbuf,
    bsend,
    brecv,
    ssout,
    ssin,
    readbuf,
    cbuf,
    psend,
    dbuf,
    acc_gu,
    ebuf,
    acc_down,
    fsend,
    frecv,
    local_sem,
    a1_send,
    a1_recv,
    a2_send,
    a2_recv,
    ss_sem,
    b_send,
    b_recv,
    c_send,
    c_fwd,
    c_recv,
    d1_send,
    d1_recv,
    d_send,
    d_fwd,
    d_recv,
    e_send,
    e_fwd,
    e_recv,
    f_send,
    f_recv,
):
    ep = lax.axis_index("ep")
    tp = lax.axis_index("tp")
    z = tp // 2
    core = tp % 2
    other = 2 * z + 1 - core

    loads = [
        (hidden, v_hidden),
        (positions, v_pos),
        (table, v_table),
        (route_ids, v_ids),
        (route_weight, v_weight),
        (head_gain, v_head_gain),
        (mix_gain, v_mix_gain),
        (ffn_gain, v_ffn_gain),
        (query_weight, v_qkvg.at[:, pl.ds(0, 128)]),
        (key_weight, v_qkvg.at[:, pl.ds(128, 128)]),
        (value_weight, v_qkvg.at[:, pl.ds(256, 128)]),
        (gate_weight, v_qkvg.at[:, pl.ds(384, 128)]),
        (ret_state, v_state),
        (out_weight, v_out),
        (expert_gate, v_gu.at[:, :, pl.ds(0, 128)]),
        (expert_up, v_gu.at[:, :, pl.ds(128, 128)]),
        (expert_down, v_down),
    ]
    copies = [pltpu.make_async_copy(src, dst, local_sem.at[i]) for i, (src, dst) in enumerate(loads)]
    for copy in copies[:12]:
        copy.start()

    barrier = pltpu.get_barrier_semaphore()

    def greet_plane(i, carry):
        peer = (ep + i) % NEP
        pl.semaphore_signal(barrier, inc=1, device_id=(peer, tp), device_id_type=MESH)
        pl.semaphore_signal(barrier, inc=1, device_id=(peer, other), device_id_type=MESH)
        return carry

    def greet_ring(i, carry):
        peer = 2 * ((z + i) % NZ) + core
        pl.semaphore_signal(barrier, inc=1, device_id=(ep, peer), device_id_type=MESH)
        return carry

    lax.fori_loop(1, NEP, greet_plane, 0)
    lax.fori_loop(1, NZ, greet_ring, 0)
    pl.semaphore_signal(barrier, inc=1, device_id=(ep, other), device_id_type=MESH)
    for copy in copies[12:]:
        copy.start()
    for copy in copies[:8]:
        copy.wait()

    eye = (
        lax.broadcasted_iota(jnp.int32, (ROWS, 128), 0)
        == lax.broadcasted_iota(jnp.int32, (ROWS, 128), 1)
    )

    inverse = v_table[HEADS : HEADS + 1, :]
    angle = v_pos[...].astype(F32) * inverse
    cosine = jnp.cos(angle)
    sine = jnp.sin(angle)
    lane = lax.broadcasted_iota(jnp.int32, (ROWS, 128), 1)
    sine = jnp.where(lane < HEAD // 2, -sine, sine)

    slot_expert = lane // 4
    first = v_ids[:, 0:1] == slot_expert
    second = v_ids[:, 1:2] == slot_expert
    named = jnp.where(first | second, 1.0, 0.0).astype(F32)
    earlier = jnp.where(
        lax.broadcasted_iota(jnp.int32, (ROWS, ROWS), 0)
        > lax.broadcasted_iota(jnp.int32, (ROWS, ROWS), 1),
        1.0,
        0.0,
    ).astype(BF16)
    ranks = jnp.dot(earlier, named.astype(BF16), preferred_element_type=F32)
    placed = jnp.where(ranks == (lane % 4).astype(F32), named, 0.0)
    combine = placed * jnp.where(first, v_weight[:, 0:1], v_weight[:, 1:2])
    del eye

    pl.semaphore_wait(barrier, 2 * (NEP - 1) + (NZ - 1) + 1)

    def copy_to(src, dst, send_sem, recv_sem, to_ep, to_tp):
        return pltpu.make_async_remote_copy(
            src_ref=src,
            dst_ref=dst,
            send_sem=send_sem,
            recv_sem=recv_sem,
            device_id=(to_ep, to_tp),
            device_id_type=MESH,
        )

    def a1_copy(i, slot):
        peer = 2 * ((z + ring_offset(i)) % NZ) + core
        return copy_to(v_hidden, agbuf.at[slot], a1_send.at[i], a1_recv.at[slot], ep, peer)

    def a1_start(i, carry):
        a1_copy(NZ - 2 - i, z).start()
        return carry

    lax.fori_loop(0, NZ - 1, a1_start, 0)

    def a2_copy(src, row, cc):
        return copy_to(
            src, xbuf.at[ep], a2_send.at[row, cc], a2_recv.at[ep], 2 * row + core, 2 * z + cc
        )

    def a2_from(src, row):
        target = 2 * row + core
        for cc in range(2):
            mine = (target == ep) & (cc == core)

            @pl.when(jnp.logical_not(mine))
            def _():
                a2_copy(src, row, cc).start()

            @pl.when(mine)
            def _():
                xbuf[pl.ds(ep, 1)] = src[...].reshape(1, ROWS, COLS)

    agbuf[pl.ds(z, 1)] = v_hidden[...].reshape(1, ROWS, COLS)
    a2_from(v_hidden, z)

    def a2_start(i, carry):
        row = (z + ring_offset(i)) % NZ
        a1_copy(i, row).wait_recv()
        a2_from(agbuf.at[row], row)
        return carry

    lax.fori_loop(0, NZ - 1, a2_start, 0)

    def square(i, total):
        part = agbuf[pl.ds(i, 1)].reshape(ROWS, COLS).astype(F32)
        part = part * part
        return total + part[:, :128] + part[:, 128:]

    ssout[...] = lax.fori_loop(0, NZ, square, jnp.zeros((ROWS, 128), F32))
    ss_copy = copy_to(ssout, ssin, ss_sem.at[0], ss_sem.at[1], ep, other)
    ss_copy.start()

    for copy in copies[8:12]:
        copy.wait()
    mix_row = v_mix_gain[:, pl.ds(pl.multiple_of(ep * COLS, COLS), COLS)]

    def plane_row(i):
        step = i + (i // 2) * (5 - 2 * i)
        return (ep // 4 + step) % 4

    def b_copy(slot, peer):
        return copy_to(bsend.at[peer], brecv.at[slot], b_send.at[peer], b_recv.at[slot], peer, tp)

    def b_rows(i, carry):
        row = plane_row(i)
        for k in range(4):
            peer = 4 * row + k

            @pl.when((peer != ep) | (ep % 2 != core))
            def _():
                copy_to(
                    v_hidden, xbuf.at[peer], a2_send.at[0, 0], a2_recv.at[peer], ep, other
                ).wait_recv()

        rows = xbuf[pl.ds(4 * row, 4)].astype(F32) * mix_row.reshape(1, 1, COLS)
        rows = rows.reshape(4 * ROWS, COLS).astype(BF16)
        sums = jnp.dot(rows, v_qkvg[...], preferred_element_type=F32)
        bsend[pl.ds(4 * row, 4)] = sums.reshape(4, ROWS, 512).astype(BF16)
        for k in range(4):
            peer = 4 * row + k

            @pl.when(peer != ep)
            def _():
                b_copy(ep, peer).start()

        return carry

    lax.fori_loop(0, 4, b_rows, 0)
    brecv[pl.ds(ep, 1)] = bsend[pl.ds(ep, 1)]

    ss_copy.wait_recv()
    square_sum = jnp.sum(ssout[...] + ssin[...], axis=-1, keepdims=True)
    factor = lax.rsqrt(square_sum * (1.0 / D) + EPS)

    def b_sum(i, total):
        row = plane_row(i)
        for k in range(4):
            peer = 4 * row + k

            @pl.when(peer != ep)
            def _():
                b_copy(peer, peer).wait_recv()

        part = brecv[pl.ds(4 * row, 4)].astype(F32)
        return total + ((part[0] + part[1]) + (part[2] + part[3]))

    joined = lax.fori_loop(0, 4, b_sum, jnp.zeros((ROWS, 512), F32))
    joined = (joined * factor).astype(BF16).astype(F32)

    def rotate(values):
        return values * cosine + pltpu.roll(values, HEAD // 2, 1) * sine

    rotated_query = rotate(joined[:, :128])
    rotated_key = rotate(joined[:, 128:256]) * HEAD ** (-0.5)
    value = joined[:, 256:384]
    gate_rows = joined[:, 384:]
    decay = v_table[pl.ds(tp, 1), :]
    readbuf[0] = rotated_query
    readbuf[1] = rotated_key
    readbuf[2] = value
    copies[12].wait()

    def retain(group, carry):
        at = pl.ds(pl.multiple_of(8 * group, 8), 8)
        query_columns = readbuf[0, at, :].T
        key_columns = readbuf[1, at, :].T
        values = readbuf[2, at, :]
        reads = []
        for k in range(8):
            state = (
                decay * v_state[8 * group + k, 0] + key_columns[:, k : k + 1] * values[k : k + 1, :]
            )
            v_state[8 * group + k, 0] = state
            reads.append(jnp.sum(query_columns[:, k : k + 1] * state, axis=0, keepdims=True))
        readbuf[3, at, :] = jnp.concatenate(reads, axis=0)
        return carry

    lax.fori_loop(0, ROWS // 8, retain, 0)
    state_out = pltpu.make_async_copy(v_state, next_state, local_sem.at[12])
    state_out.start()
    read = readbuf[3]
    centered = read - jnp.mean(read, axis=-1, keepdims=True)
    normal = centered * lax.rsqrt(jnp.mean(centered * centered, axis=-1, keepdims=True) + EPS)
    mixed = normal * v_head_gain[...] * jax.nn.silu(gate_rows)
    cbuf[pl.ds(tp, 1)] = mixed.astype(BF16).reshape(1, ROWS, HEAD)

    def gather(buf, send_sem, fwd_sem, recv_sem, consume):
        def direct(i, slot):
            peer = 2 * ((z + ring_offset(i)) % NZ) + core
            return copy_to(buf.at[slot], buf.at[slot], send_sem.at[i], recv_sem.at[slot], ep, peer)

        def forward(row, slot):
            return copy_to(
                buf.at[slot], buf.at[slot], fwd_sem.at[row], recv_sem.at[slot], ep, other
            )

        def begin(i, carry):
            direct(NZ - 2 - i, tp).start()
            return carry

        lax.fori_loop(0, NZ - 1, begin, 0)
        forward(z, tp).start()

        def step(i, carry):
            @pl.when(i < NZ - 1)
            def _():
                row = (z + ring_offset(i)) % NZ
                direct(0, 2 * row + core).wait_recv()
                forward(row, 2 * row + core).start()

            before = lax.select(i > 0, (z + ring_offset(lax.max(i - 1, 0))) % NZ, z)
            forward(before, 2 * before + 1 - core).wait_recv()
            consume(before, i == 0)
            return carry

        lax.fori_loop(0, NZ, step, 0)

        def finish():
            def one(i, carry):
                direct(i, tp).wait_send()
                forward((z + ring_offset(i)) % NZ, tp).wait_send()
                return carry

            lax.fori_loop(0, NZ - 1, one, 0)
            forward(z, tp).wait_send()

        return finish

    copies[13].wait()
    projected = readbuf.at[pl.ds(0, 2)]

    def project(row, first_step):
        pair = cbuf[pl.ds(2 * row, 2)].astype(F32)
        block = jnp.concatenate([pair[0], pair[1]], axis=1).astype(BF16)
        part = jnp.dot(
            block,
            v_out[pl.ds(pl.multiple_of(row * COLS, COLS), COLS), :],
            preferred_element_type=F32,
        )

        @pl.when(first_step)
        def _():
            projected[0] = part[:, :128]
            projected[1] = part[:, 128:]

        @pl.when(jnp.logical_not(first_step))
        def _():
            projected[0] += part[:, :128]
            projected[1] += part[:, 128:]

    finish_c = gather(cbuf, c_send, c_fwd, c_recv, project)
    own = v_hidden[...].astype(F32)
    after = (own + jnp.concatenate([projected[0], projected[1]], axis=1)).astype(BF16)

    packed = lax.dot_general(
        placed.astype(BF16), after, (((0,), (0,)), ((), ())), preferred_element_type=F32
    )

    def halves_below(array):
        parts = [array[:, :128].reshape(NEP, 8, 128), array[:, 128:].reshape(NEP, 8, 128)]
        return jnp.concatenate(parts, axis=1)

    def halves_beside(array):
        array = array.astype(F32)
        return array[:, :8].reshape(SLOTS, 128), array[:, 8:].reshape(SLOTS, 128)

    psend[...] = halves_below(packed).astype(BF16)

    def d1_copy(peer, source):
        return copy_to(
            psend.at[peer], dbuf.at[tp, source], d1_send.at[peer], d1_recv.at[source], peer, tp
        )

    def d1_start(i, carry):
        d1_copy((ep + i) % NEP, ep).start()
        return carry

    lax.fori_loop(1, NEP, d1_start, 0)
    dbuf[pl.ds(tp, 1), pl.ds(ep, 1)] = psend[pl.ds(ep, 1)].reshape(1, 1, 16, 128)

    def d1_wait(i, carry):
        peer = (ep + i) % NEP
        d1_copy(peer, peer).wait_recv()
        return carry

    lax.fori_loop(1, NEP, d1_wait, 0)
    copies[14].wait()
    copies[15].wait()

    square_of = acc_gu.at[2]

    def lift(row, first_step):
        @pl.when(first_step)
        def _():
            acc_gu[...] = jnp.zeros_like(acc_gu)

        for k in range(2):
            slot = 2 * row + k
            at = pl.multiple_of(slot * COLS, COLS)
            low, high = halves_beside(dbuf[pl.ds(slot, 1)].reshape(NEP, 16, 128))
            square_of[:, :128] += low * low + high * high
            both = jnp.concatenate([low, high], axis=1) * v_ffn_gain[:, pl.ds(at, COLS)]
            both = both.astype(BF16)
            for j in range(2):
                acc_gu[j] += jnp.dot(both, v_gu[j, pl.ds(at, COLS), :], preferred_element_type=F32)

    finish_d = gather(dbuf, d_send, d_fwd, d_recv, lift)
    inner = lax.rsqrt(
        jnp.sum(square_of[:, :128], axis=-1, keepdims=True) * (1.0 / D) + EPS
    )
    own_expert = lax.broadcasted_iota(jnp.int32, (SLOTS, COLS), 0) % 8 < 4
    chosen = jnp.where(own_expert, acc_gu[0], acc_gu[1]) * inner
    activated = jax.nn.silu(chosen[:, :128]) * chosen[:, 128:]
    ebuf[pl.ds(tp, 1)] = activated.astype(BF16).reshape(1, SLOTS, 128)
    copies[16].wait()

    def lower(row, first_step):
        @pl.when(first_step)
        def _():
            acc_down[...] = jnp.zeros_like(acc_down)

        pair = ebuf[pl.ds(2 * row, 2)]
        both = jnp.concatenate([pair[0], pair[1]], axis=1)
        at = pl.multiple_of(row * COLS, COLS)
        for j in range(2):
            acc_down[j] += jnp.dot(both, v_down[j, pl.ds(at, COLS), :], preferred_element_type=F32)

    finish_e = gather(ebuf, e_send, e_fwd, e_recv, lower)
    result = jnp.where(own_expert, acc_down[0], acc_down[1])

    fsend[...] = halves_below(result).astype(BF16)

    def f_copy(peer, source):
        return copy_to(
            fsend.at[peer], frecv.at[source], f_send.at[peer], f_recv.at[source], peer, tp
        )

    def f_start(i, carry):
        f_copy((ep + i) % NEP, ep).start()
        return carry

    lax.fori_loop(1, NEP, f_start, 0)
    frecv[pl.ds(ep, 1)] = fsend[pl.ds(ep, 1)]

    def sent_ring(i, carry):
        a1_copy(i, z).wait_send()
        return carry

    lax.fori_loop(0, NZ - 1, sent_ring, 0)

    def sent_a2(row, carry):
        for cc in range(2):

            @pl.when((2 * row + core != ep) | (cc != core))
            def _():
                a2_copy(v_hidden, row, cc).wait_send()

        return carry

    lax.fori_loop(0, NZ, sent_a2, 0)
    ss_copy.wait_send()

    def sent_plane(i, carry):
        peer = (ep + i) % NEP
        b_copy(ep, peer).wait_send()
        d1_copy(peer, ep).wait_send()
        return carry

    lax.fori_loop(1, NEP, sent_plane, 0)
    finish_c()
    finish_d()
    finish_e()

    def f_wait(i, carry):
        peer = (ep + i) % NEP
        f_copy(peer, peer).wait_recv()
        return carry

    lax.fori_loop(1, NEP, f_wait, 0)
    back = jnp.concatenate(halves_beside(frecv[...]), axis=1)
    weighted = jnp.dot(
        combine, back, preferred_element_type=F32, precision=lax.Precision.HIGHEST
    )
    updated[...] = (after.astype(F32) + weighted).astype(BF16)

    def f_sent(i, carry):
        f_copy((ep + i) % NEP, ep).wait_send()
        return carry

    lax.fori_loop(1, NEP, f_sent, 0)
    state_out.wait()


def per_device(
    hidden,
    positions,
    ret_state,
    query_weight,
    key_weight,
    value_weight,
    gate_weight,
    head_gain,
    out_weight,
    mix_gain,
    ffn_gain,
    expert_gate,
    expert_up,
    expert_down,
    route_ids,
    route_weight,
):
    dma = pltpu.SemaphoreType.DMA
    vmem = pltpu.VMEM
    anywhere = pl.BlockSpec(memory_space=pl.ANY)
    return pl.pallas_call(
        body,
        out_shape=(
            jax.ShapeDtypeStruct((ROWS, COLS), BF16),
            jax.ShapeDtypeStruct(ret_state.shape, F32),
        ),
        in_specs=[anywhere] * 17,
        out_specs=(pl.BlockSpec(memory_space=pltpu.VMEM), anywhere),
        scratch_shapes=[
            vmem((ROWS, COLS), BF16),
            vmem((ROWS, 1), jnp.int32),
            vmem((ROWS, 1, HEAD, HEAD), F32),
            vmem((COLS, 512), BF16),
            vmem((1, HEAD), F32),
            vmem((RD, COLS), BF16),
            vmem((1, D), F32),
            vmem((1, D), F32),
            vmem((2, D, COLS), BF16),
            vmem((2, RD, COLS), BF16),
            vmem((ROWS, 2), jnp.int32),
            vmem((ROWS, 2), F32),
            vmem((24, 128), F32),
            vmem((NZ, ROWS, COLS), BF16),
            vmem((NEP, ROWS, COLS), BF16),
            vmem((NEP, ROWS, 512), BF16),
            vmem((NEP, ROWS, 512), BF16),
            vmem((ROWS, 128), F32),
            vmem((ROWS, 128), F32),
            vmem((4, ROWS, HEAD), F32),
            vmem((NTP, ROWS, HEAD), BF16),
            vmem((NEP, 16, 128), BF16),
            vmem((NTP, NEP, 16, 128), BF16),
            vmem((3, SLOTS, COLS), F32),
            vmem((NTP, SLOTS, 128), BF16),
            vmem((2, SLOTS, COLS), F32),
            vmem((NEP, 16, 128), BF16),
            vmem((NEP, 16, 128), BF16),
            dma((17,)),
            dma((NZ,)),
            dma((NZ,)),
            dma((NZ, 2)),
            dma((NEP,)),
            dma((2,)),
            dma((NEP,)),
            dma((NEP,)),
            dma((NZ,)),
            dma((NZ,)),
            dma((NTP,)),
            dma((NEP,)),
            dma((NEP,)),
            dma((NZ,)),
            dma((NZ,)),
            dma((NTP,)),
            dma((NZ,)),
            dma((NZ,)),
            dma((NTP,)),
            dma((NEP,)),
            dma((NEP,)),
        ],
        compiler_params=pltpu.CompilerParams(
            collective_id=0, has_side_effects=True, vmem_limit_bytes=48 * 1024 * 1024
        ),
    )(
        hidden,
        positions.reshape(ROWS, 1),
        ret_state,
        query_weight,
        key_weight,
        value_weight,
        gate_weight,
        head_gain.reshape(1, HEAD),
        out_weight,
        mix_gain.reshape(1, D),
        ffn_gain.reshape(1, D),
        expert_gate,
        expert_up,
        expert_down,
        route_ids,
        route_weight,
        jnp.asarray(constants()),
    )


def solution(mesh):
    return jax.shard_map(
        per_device,
        mesh=mesh,
        in_specs=(
            P("ep", "tp"),
            P("ep"),
            P("ep", "tp", None, None),
            P("ep", "tp"),
            P("ep", "tp"),
            P("ep", "tp"),
            P("ep", "tp"),
            P("tp"),
            P(None, "tp"),
            P(),
            P(),
            P("ep", None, "tp"),
            P("ep", None, "tp"),
            P("ep", None, "tp"),
            P("ep", None),
            P("ep", None),
        ),
        out_specs=(P("ep", "tp"), P("ep", "tp", None, None)),
        check_vma=False,
    )
```

time: 168 us -> 106 us (0.63)
  Pallas kernels: 0 us -> 86.8 us
  waiting for transfers between devices: 72.8 us -> 0 us
  blocking collectives: 38 us -> 0 us
  starting transfers between devices: 30.6 us -> 0 us
  matrix products: 7.99 us -> 0 us
  local copies, waits for them, and re-layouts: 10.9 us -> 17.7 us
  other arithmetic: 5.93 us -> 0 us
    pallas_call x0 -> x1, Pallas kernels: none -> 86.8 us  [per_device(): pl.pallas_call(body, out_shape=(jax.ShapeDtypeStruct((ROWS, COLS), BF16),...]
    all_to_all x6 -> x0, waiting for transfers between devices: 72.8 us -> none  [the longest x4 50.9 us: from_everyone(): lax.all_to_all(jnp.broadcast_to(array[None], (size, *array.shape)), axis,...]
    all_to_all x2 -> x0, blocking collectives: 38 us -> none  [the longest x1 22 us: per_device(): lax.all_to_all(packed.reshape(peers, local_experts, capacity, source.shap...]
    all_to_all x6 -> x0, starting transfers between devices: 30.6 us -> none  [the longest x4 23.4 us: from_everyone(): lax.all_to_all(jnp.broadcast_to(array[None], (size, *array.shape)), axis,...]
    unnamed x28, local copies, waits for them, and re-layouts: 0.26 us -> 16.9 us
    dot_general x7 -> x0, matrix products: 7.99 us -> none  [the longest x1 2.6 us: retain(): read = jnp.einsum('bhd,bhde->bhe', rotated_query, next_state)]
    broadcast_in_dim x4 -> x0, local copies, waits for them, and re-layouts: 3.98 us -> none  [from_everyone(): jnp.broadcast_to(array[None], (size, *array.shape))]
    add x2 -> x0, other arithmetic: 3.29 us -> none  [the longest x1 3.28 us: retain(): decay[None, :, None, None] * ret_state]
  transfers between devices with their start and end apart: 6 -> 0, of which waited for: 6 -> 0; matrix products, arithmetic and copies ran while one was open for 3% -> 0% of each run, Pallas kernels for 0% -> 0%
where the time goes in v1:
time: 106 us; the launch traced here: 105 us
  Pallas kernels  86.8 us (82%)
  local copies, waits for them, and re-layouts  17.7 us (17%)
    pallas_call x1, Pallas kernels, per_device(): pl.pallas_call(body, out_shape=(jax.ShapeDtypeStruct((ROWS, COLS), BF16),...  86.8 us
    unnamed x28, local copies, waits for them, and re-layouts  16.9 us

profile of v1, /device:TPU:1, one launch (start us, length us, event | category | flops | bytes accessed | tf_op | source)
XLA Modules:
  0.0 105.2 jit_solution(14425095900111086047)
XLA Ops:
  0.6 0.7 copy.19.positions
  1.4 0.8 copy.20.route_ids
  2.1 0.8 copy.21.route_weight
  2.9 0.0 copy-start
  2.9 1.6 %copy-done = bf16[2,4096,128]{2,1,0:T(8,128)(2,1)S(1)} copy-done((bf16[2,4096,128]{2,1,0:T(8,128)(2,1)S(1)}, bf16[2,4096,128]{2,1,0:T(8,128)(2,1)}, u32[]{:S(2)}) %copy-start) | copy-done | bytes 2097176
  4.5 0.0 copy-start.1
  4.5 1.6 %copy-done.1 = bf16[2,4096,128]{2,1,0:T(8,128)(2,1)S(1)} copy-done((bf16[2,4096,128]{2,1,0:T(8,128)(2,1)S(1)}, bf16[2,4096,128]{2,1,0:T(8,128)(2,1)}, u32[]{:S(2)}) %copy-start.1) | copy-done | bytes 2097176
  6.1 0.0 copy-start.2
  6.1 1.2 %copy-done.2 = bf16[2048,256]{1,0:T(8,128)(2,1)S(1)} copy-done((bf16[2048,256]{1,0:T(8,128)(2,1)S(1)}, bf16[2048,256]{1,0:T(8,128)(2,1)}, u32[]{:S(2)}) %copy-start.2) | copy-done | bytes 1048600
  7.3 0.0 copy-start.3
  7.3 0.8 copy-done.3
  8.1 0.0 copy-start.4
  8.1 0.8 copy-done.4
  9.0 0.0 copy-start.5
  9.0 0.8 copy-done.5
  9.8 0.0 copy-start.6
  9.8 0.8 copy-done.6
  10.7 0.0 copy-start.7
  10.7 0.7 copy-done.7
  11.4 0.0 copy-start.8
  11.4 0.7 copy-done.8
  12.1 0.0 copy-start.9
  12.1 0.7 copy-done.9
  12.8 0.0 copy-start.10
  12.8 0.7 copy-done.10
  13.5 0.0 copy-start.11
  13.5 0.7 copy-done.11
  14.2 86.8 %shard_map.176 = (bf16[40,256]{1,0:T(8,128)(2,1)S(1)}, f32[40,1,128,128]{3,2,1,0:T(8,128)}) custom-call(bf16[40,256]{1,0:T(8,128)(2,1)S(1)} %copy-done.7, s32[40,1]{1,0:T(8,128)S(1)} %copy.19.positions, f32[40,1,128,128]{3,2,1,0:T(8,128)} %ret_state.1, bf16[256,128]{1,0:T(8,128)(2,1)S(1)} %copy-done.3, bf16[256,128]{1,0:T(8,128)(2,1)S(1)} %copy-done.4, ...), custom_call_target="tpu_custom_call" | custom-call | tf_op jit(solution)/shard_map/pallas_call | solution.py:570
  101.0 0.6 copy.24
  101.6 3.5 %copy.25 = f32[40,1,128,128]{3,2,1,0:T(8,128)} copy(f32[40,1,128,128]{3,2,1,0:T(8,128)} %get-tuple-element.5) | data formatting | bytes 5242880
Async XLA Ops:
  2.9 1.6 %copy-start = (bf16[2,4096,128]{2,1,0:T(8,128)(2,1)S(1)}, bf16[2,4096,128]{2,1,0:T(8,128)(2,1)}, u32[]{:S(2)}) copy-start(bf16[2,4096,128]{2,1,0:T(8,128)(2,1)} %expert_gate.1) | copy-start | bytes 6291460
  4.5 1.6 %copy-start.1 = (bf16[2,4096,128]{2,1,0:T(8,128)(2,1)S(1)}, bf16[2,4096,128]{2,1,0:T(8,128)(2,1)}, u32[]{:S(2)}) copy-start(bf16[2,4096,128]{2,1,0:T(8,128)(2,1)} %expert_up.1) | copy-start | bytes 6291460
  6.1 1.2 %copy-start.2 = (bf16[2048,256]{1,0:T(8,128)(2,1)S(1)}, bf16[2048,256]{1,0:T(8,128)(2,1)}, u32[]{:S(2)}) copy-start(bf16[2048,256]{1,0:T(8,128)(2,1)} %out_weight.1) | copy-start | bytes 3145732
  7.3 0.8 copy-start.3
  8.1 0.8 copy-start.4
  9.0 0.8 copy-start.5
  9.8 0.8 copy-start.6
  10.7 0.7 copy-start.7
  11.4 0.7 copy-start.8
  12.1 0.7 copy-start.9
  12.8 0.7 copy-start.10
  13.5 0.7 copy-start.11

commit v2 on v1

--- a/solution.py
+++ b/solution.py
@@ -21,6 +21,7 @@
 NTP = 16
 NZ = 8
 SLOTS = 128
+GROUPS_OF_ROWS = ROWS // 8
 EPS = 1e-06
 
 
@@ -31,6 +32,20 @@
     inverse = 10000.0 ** (-np.arange(0, HEAD, 2, dtype=np.float64) / HEAD)
     table[HEADS] = np.concatenate([inverse, inverse])
     return table.astype(np.float32)
+
+
+TRACE = False
+_open = []
+
+
+def mark(name):
+    if not TRACE:
+        return
+    while _open:
+        _open.pop().__exit__(None, None, None)
+    if name:
+        _open.append(jax.named_scope(name))
+        _open[-1].__enter__()
 
 
 def ring_offset(i):
@@ -57,7 +72,7 @@
     route_weight,
     table,
     updated,
-    next_state,
+    state_parts,
     v_hidden,
     v_pos,
     v_state,
@@ -79,6 +94,7 @@
     ssin,
     readbuf,
     cbuf,
+    afters,
     psend,
     dbuf,
     acc_gu,
@@ -97,11 +113,12 @@
     c_send,
     c_fwd,
     c_recv,
-    d1_send,
-    d1_recv,
+    g_send,
+    g_recv,
     d_send,
     d_fwd,
     d_recv,
+    d_other,
     e_send,
     e_fwd,
     e_recv,
@@ -114,6 +131,7 @@
     core = tp % 2
     other = 2 * z + 1 - core
 
+    mark("load")
     loads = [
         (hidden, v_hidden),
         (positions, v_pos),
@@ -158,33 +176,31 @@
     for copy in copies[:8]:
         copy.wait()
 
-    eye = (
-        lax.broadcasted_iota(jnp.int32, (ROWS, 128), 0)
-        == lax.broadcasted_iota(jnp.int32, (ROWS, 128), 1)
-    )
+    mark("prep")
+    token = lax.broadcasted_iota(jnp.int32, (ROWS, ROWS), 0)
+    other_token = lax.broadcasted_iota(jnp.int32, (ROWS, ROWS), 1)
+
+    def column(row):
+        return jnp.sum(jnp.where(token == other_token, row.astype(F32), 0.0), axis=1, keepdims=True)
 
     inverse = v_table[HEADS : HEADS + 1, :]
-    angle = v_pos[...].astype(F32) * inverse
+    angle = column(v_pos[...]) * inverse
     cosine = jnp.cos(angle)
     sine = jnp.sin(angle)
     lane = lax.broadcasted_iota(jnp.int32, (ROWS, 128), 1)
     sine = jnp.where(lane < HEAD // 2, -sine, sine)
 
     slot_expert = lane // 4
-    first = v_ids[:, 0:1] == slot_expert
-    second = v_ids[:, 1:2] == slot_expert
+    slot_expert = slot_expert.astype(F32)
+    first = column(v_ids[0:1, :]) == slot_expert
+    second = column(v_ids[1:2, :]) == slot_expert
     named = jnp.where(first | second, 1.0, 0.0).astype(F32)
-    earlier = jnp.where(
-        lax.broadcasted_iota(jnp.int32, (ROWS, ROWS), 0)
-        > lax.broadcasted_iota(jnp.int32, (ROWS, ROWS), 1),
-        1.0,
-        0.0,
-    ).astype(BF16)
+    earlier = jnp.where(token > other_token, 1.0, 0.0).astype(BF16)
     ranks = jnp.dot(earlier, named.astype(BF16), preferred_element_type=F32)
     placed = jnp.where(ranks == (lane % 4).astype(F32), named, 0.0)
-    combine = placed * jnp.where(first, v_weight[:, 0:1], v_weight[:, 1:2])
-    del eye
-
+    combine = placed * jnp.where(first, column(v_weight[0:1, :]), column(v_weight[1:2, :]))
+
+    mark("barrier")
     pl.semaphore_wait(barrier, 2 * (NEP - 1) + (NZ - 1) + 1)
 
     def copy_to(src, dst, send_sem, recv_sem, to_ep, to_tp):
@@ -205,6 +221,7 @@
         a1_copy(NZ - 2 - i, z).start()
         return carry
 
+    mark("a1_issue")
     lax.fori_loop(0, NZ - 1, a1_start, 0)
 
     def a2_copy(src, row, cc):
@@ -234,8 +251,10 @@
         a2_from(agbuf.at[row], row)
         return carry
 
+    mark("a1_wait_a2_issue")
     lax.fori_loop(0, NZ - 1, a2_start, 0)
 
+    mark("ss")
     def square(i, total):
         part = agbuf[pl.ds(i, 1)].reshape(ROWS, COLS).astype(F32)
         part = part * part
@@ -248,6 +267,12 @@
     for copy in copies[8:12]:
         copy.wait()
     mix_row = v_mix_gain[:, pl.ds(pl.multiple_of(ep * COLS, COLS), COLS)]
+
+    def plane_peer(i):
+        down, along = i // 4, i % 4
+        down = down + (down // 2) * (5 - 2 * down)
+        along = along + (along // 2) * (5 - 2 * along)
+        return ((ep // 4 + down) % 4) * 4 + (ep + along) % 4
 
     def plane_row(i):
         step = i + (i // 2) * (5 - 2 * i)
@@ -280,9 +305,11 @@
 
         return carry
 
+    mark("b_rows")
     lax.fori_loop(0, 4, b_rows, 0)
     brecv[pl.ds(ep, 1)] = bsend[pl.ds(ep, 1)]
 
+    mark("ss_wait")
     ss_copy.wait_recv()
     square_sum = jnp.sum(ssout[...] + ssin[...], axis=-1, keepdims=True)
     factor = lax.rsqrt(square_sum * (1.0 / D) + EPS)
@@ -299,9 +326,11 @@
         part = brecv[pl.ds(4 * row, 4)].astype(F32)
         return total + ((part[0] + part[1]) + (part[2] + part[3]))
 
+    mark("b_sum")
     joined = lax.fori_loop(0, 4, b_sum, jnp.zeros((ROWS, 512), F32))
     joined = (joined * factor).astype(BF16).astype(F32)
 
+    mark("rot")
     def rotate(values):
         return values * cosine + pltpu.roll(values, HEAD // 2, 1) * sine
 
@@ -313,6 +342,9 @@
     readbuf[0] = rotated_query
     readbuf[1] = rotated_key
     readbuf[2] = value
+    state_parts[0] = rotated_key
+    state_parts[1] = value
+    mark("retain")
     copies[12].wait()
 
     def retain(group, carry):
@@ -325,14 +357,12 @@
             state = (
                 decay * v_state[8 * group + k, 0] + key_columns[:, k : k + 1] * values[k : k + 1, :]
             )
-            v_state[8 * group + k, 0] = state
             reads.append(jnp.sum(query_columns[:, k : k + 1] * state, axis=0, keepdims=True))
         readbuf[3, at, :] = jnp.concatenate(reads, axis=0)
         return carry
 
     lax.fori_loop(0, ROWS // 8, retain, 0)
-    state_out = pltpu.make_async_copy(v_state, next_state, local_sem.at[12])
-    state_out.start()
+    mark("groupnorm")
     read = readbuf[3]
     centered = read - jnp.mean(read, axis=-1, keepdims=True)
     normal = centered * lax.rsqrt(jnp.mean(centered * centered, axis=-1, keepdims=True) + EPS)
@@ -403,13 +433,22 @@
             projected[0] += part[:, :128]
             projected[1] += part[:, 128:]
 
+    mark("c_gather")
     finish_c = gather(cbuf, c_send, c_fwd, c_recv, project)
+    mark("after_pack")
     own = v_hidden[...].astype(F32)
     after = (own + jnp.concatenate([projected[0], projected[1]], axis=1)).astype(BF16)
-
-    packed = lax.dot_general(
-        placed.astype(BF16), after, (((0,), (0,)), ((), ())), preferred_element_type=F32
-    )
+    afters[pl.ds(z, 1)] = after.reshape(1, ROWS, COLS)
+
+    def g_copy(i, slot):
+        peer = 2 * ((z + ring_offset(i)) % NZ) + core
+        return copy_to(afters.at[z], afters.at[slot], g_send.at[i], g_recv.at[slot], ep, peer)
+
+    def g_start(i, carry):
+        g_copy(NZ - 2 - i, z).start()
+        return carry
+
+    lax.fori_loop(0, NZ - 1, g_start, 0)
 
     def halves_below(array):
         parts = [array[:, :128].reshape(NEP, 8, 128), array[:, 128:].reshape(NEP, 8, 128)]
@@ -419,47 +458,85 @@
         array = array.astype(F32)
         return array[:, :8].reshape(SLOTS, 128), array[:, 8:].reshape(SLOTS, 128)
 
-    psend[...] = halves_below(packed).astype(BF16)
-
-    def d1_copy(peer, source):
+    placing = placed.astype(BF16)
+
+    def pack(row):
+        packed = lax.dot_general(
+            placing,
+            afters[pl.ds(row, 1)].reshape(ROWS, COLS),
+            (((0,), (0,)), ((), ())),
+            preferred_element_type=F32,
+        )
+        psend[:, pl.ds(row, 1)] = halves_below(packed).astype(BF16).reshape(NEP, 1, 16, 128)
+
+    pack(z)
+
+    def pack_next(i, carry):
+        row = (z + ring_offset(i)) % NZ
+        g_copy(i, row).wait_recv()
+        pack(row)
+        return carry
+
+    mark("after_gather")
+    lax.fori_loop(0, NZ - 1, pack_next, 0)
+
+    def d_copy(peer, source):
         return copy_to(
-            psend.at[peer], dbuf.at[tp, source], d1_send.at[peer], d1_recv.at[source], peer, tp
+            psend.at[peer], dbuf.at[core, source], d_send.at[peer], d_recv.at[source], peer, tp
         )
 
-    def d1_start(i, carry):
-        d1_copy((ep + i) % NEP, ep).start()
-        return carry
-
-    lax.fori_loop(1, NEP, d1_start, 0)
-    dbuf[pl.ds(tp, 1), pl.ds(ep, 1)] = psend[pl.ds(ep, 1)].reshape(1, 1, 16, 128)
-
-    def d1_wait(i, carry):
-        peer = (ep + i) % NEP
-        d1_copy(peer, peer).wait_recv()
-        return carry
-
-    lax.fori_loop(1, NEP, d1_wait, 0)
+    def d_forward(parity, source):
+        block = dbuf.at[parity, source]
+        return copy_to(block, block, d_fwd.at[source], d_other.at[source], ep, other)
+
+    def d_start(i, carry):
+        d_copy(plane_peer(NEP - 1 - i), ep).start()
+        return carry
+
+    mark("d_issue")
+    lax.fori_loop(0, NEP - 1, d_start, 0)
+    dbuf[pl.ds(core, 1), pl.ds(ep, 1)] = psend[pl.ds(ep, 1)].reshape(1, 1, NZ, 16, 128)
+    d_forward(core, ep).start()
+
+    def d_arrive(i, carry):
+        peer = plane_peer(i)
+        d_copy(peer, peer).wait_recv()
+        d_forward(core, peer).start()
+        return carry
+
+    acc_gu[...] = jnp.zeros_like(acc_gu)
+    mark("d_wait")
+    lax.fori_loop(1, NEP, d_arrive, 0)
     copies[14].wait()
     copies[15].wait()
-
     square_of = acc_gu.at[2]
 
-    def lift(row, first_step):
-        @pl.when(first_step)
-        def _():
-            acc_gu[...] = jnp.zeros_like(acc_gu)
-
-        for k in range(2):
-            slot = 2 * row + k
-            at = pl.multiple_of(slot * COLS, COLS)
-            low, high = halves_beside(dbuf[pl.ds(slot, 1)].reshape(NEP, 16, 128))
+    def lift(parity):
+        def one(row, carry):
+            at = pl.multiple_of((2 * row + parity) * COLS, COLS)
+            block = dbuf[pl.ds(parity, 1), :, pl.ds(row, 1)].reshape(NEP, 16, 128)
+            low, high = halves_beside(block)
             square_of[:, :128] += low * low + high * high
             both = jnp.concatenate([low, high], axis=1) * v_ffn_gain[:, pl.ds(at, COLS)]
             both = both.astype(BF16)
             for j in range(2):
                 acc_gu[j] += jnp.dot(both, v_gu[j, pl.ds(at, COLS), :], preferred_element_type=F32)
-
-    finish_d = gather(dbuf, d_send, d_fwd, d_recv, lift)
+            return carry
+
+        lax.fori_loop(0, NZ, one, 0)
+
+    mark("lift_own")
+    lift(core)
+
+    def d_other_wait(source, carry):
+        d_forward(1 - core, source).wait_recv()
+        return carry
+
+    mark("lift_wait")
+    lax.fori_loop(0, NEP, d_other_wait, 0)
+    mark("lift_other")
+    lift(1 - core)
+    mark("act")
     inner = lax.rsqrt(
         jnp.sum(square_of[:, :128], axis=-1, keepdims=True) * (1.0 / D) + EPS
     )
@@ -480,7 +557,9 @@
         for j in range(2):
             acc_down[j] += jnp.dot(both, v_down[j, pl.ds(at, COLS), :], preferred_element_type=F32)
 
+    mark("e_gather")
     finish_e = gather(ebuf, e_send, e_fwd, e_recv, lower)
+    mark("result")
     result = jnp.where(own_expert, acc_down[0], acc_down[1])
 
     fsend[...] = halves_below(result).astype(BF16)
@@ -497,8 +576,10 @@
     lax.fori_loop(1, NEP, f_start, 0)
     frecv[pl.ds(ep, 1)] = fsend[pl.ds(ep, 1)]
 
+    mark("sent")
     def sent_ring(i, carry):
         a1_copy(i, z).wait_send()
+        g_copy(i, z).wait_send()
         return carry
 
     lax.fori_loop(0, NZ - 1, sent_ring, 0)
@@ -514,16 +595,17 @@
 
     lax.fori_loop(0, NZ, sent_a2, 0)
     ss_copy.wait_send()
+    d_forward(core, ep).wait_send()
 
     def sent_plane(i, carry):
         peer = (ep + i) % NEP
         b_copy(ep, peer).wait_send()
-        d1_copy(peer, ep).wait_send()
+        d_copy(peer, ep).wait_send()
+        d_forward(core, peer).wait_send()
         return carry
 
     lax.fori_loop(1, NEP, sent_plane, 0)
     finish_c()
-    finish_d()
     finish_e()
 
     def f_wait(i, carry):
@@ -531,7 +613,9 @@
         f_copy(peer, peer).wait_recv()
         return carry
 
+    mark("f_wait")
     lax.fori_loop(1, NEP, f_wait, 0)
+    mark("combine")
     back = jnp.concatenate(halves_beside(frecv[...]), axis=1)
     weighted = jnp.dot(
         combine, back, preferred_element_type=F32, precision=lax.Precision.HIGHEST
@@ -543,7 +627,52 @@
         return carry
 
     lax.fori_loop(1, NEP, f_sent, 0)
-    state_out.wait()
+    mark("")
+
+
+def state_body(
+    before, parts, table, ret_state, updated, next_state, v_updated, v_parts, v_table, v_state, sem, load, store
+):
+    copies = [
+        pltpu.make_async_copy(parts, v_parts, sem.at[0]),
+        pltpu.make_async_copy(table, v_table, sem.at[1]),
+        pltpu.make_async_copy(before, v_updated, sem.at[2]),
+    ]
+    out = pltpu.make_async_copy(v_updated, updated, sem.at[3])
+
+    def rows_in(group):
+        at = pl.ds(8 * group, 8)
+        return pltpu.make_async_copy(ret_state.at[at], v_state.at[at], load.at[group])
+
+    def rows_out(group):
+        at = pl.ds(8 * group, 8)
+        return pltpu.make_async_copy(v_state.at[at], next_state.at[at], store.at[group])
+
+    for copy in copies:
+        copy.start()
+    for group in range(GROUPS_OF_ROWS):
+        rows_in(group).start()
+    for copy in copies:
+        copy.wait()
+    out.start()
+    decay = v_table[pl.ds(lax.axis_index("tp"), 1), :]
+
+    def one(group, carry):
+        at = pl.ds(pl.multiple_of(8 * group, 8), 8)
+        key_columns = v_parts[0, at, :].T
+        values = v_parts[1, at, :]
+        rows_in(group).wait()
+        for k in range(8):
+            v_state[8 * group + k, 0] = (
+                decay * v_state[8 * group + k, 0] + key_columns[:, k : k + 1] * values[k : k + 1, :]
+            )
+        rows_out(group).start()
+        return carry
+
+    lax.fori_loop(0, GROUPS_OF_ROWS, one, 0)
+    out.wait()
+    for group in range(GROUPS_OF_ROWS):
+        rows_out(group).wait()
 
 
 def per_device(
@@ -564,20 +693,21 @@
     route_ids,
     route_weight,
 ):
+    table = jnp.asarray(constants())
     dma = pltpu.SemaphoreType.DMA
     vmem = pltpu.VMEM
-    anywhere = pl.BlockSpec(memory_space=pl.ANY)
-    return pl.pallas_call(
+    anywhere = pl.BlockSpec(memory_space=pltpu.HBM)
+    updated, parts = pl.pallas_call(
         body,
         out_shape=(
             jax.ShapeDtypeStruct((ROWS, COLS), BF16),
-            jax.ShapeDtypeStruct(ret_state.shape, F32),
+            jax.ShapeDtypeStruct((2, ROWS, HEAD), F32),
         ),
         in_specs=[anywhere] * 17,
-        out_specs=(pl.BlockSpec(memory_space=pltpu.VMEM), anywhere),
+        out_specs=(pl.BlockSpec(memory_space=pltpu.VMEM),) * 2,
         scratch_shapes=[
             vmem((ROWS, COLS), BF16),
-            vmem((ROWS, 1), jnp.int32),
+            vmem((1, ROWS), jnp.int32),
             vmem((ROWS, 1, HEAD, HEAD), F32),
             vmem((COLS, 512), BF16),
             vmem((1, HEAD), F32),
@@ -586,8 +716,8 @@
             vmem((1, D), F32),
             vmem((2, D, COLS), BF16),
             vmem((2, RD, COLS), BF16),
-            vmem((ROWS, 2), jnp.int32),
-            vmem((ROWS, 2), F32),
+            vmem((2, ROWS), jnp.int32),
+            vmem((2, ROWS), F32),
             vmem((24, 128), F32),
             vmem((NZ, ROWS, COLS), BF16),
             vmem((NEP, ROWS, COLS), BF16),
@@ -597,8 +727,9 @@
             vmem((ROWS, 128), F32),
             vmem((4, ROWS, HEAD), F32),
             vmem((NTP, ROWS, HEAD), BF16),
-            vmem((NEP, 16, 128), BF16),
-            vmem((NTP, NEP, 16, 128), BF16),
+            vmem((NZ, ROWS, COLS), BF16),
+            vmem((NEP, NZ, 16, 128), BF16),
+            vmem((2, NEP, NZ, 16, 128), BF16),
             vmem((3, SLOTS, COLS), F32),
             vmem((NTP, SLOTS, 128), BF16),
             vmem((2, SLOTS, COLS), F32),
@@ -615,11 +746,12 @@
             dma((NZ,)),
             dma((NZ,)),
             dma((NTP,)),
+            dma((NZ,)),
+            dma((NZ,)),
             dma((NEP,)),
             dma((NEP,)),
-            dma((NZ,)),
-            dma((NZ,)),
-            dma((NTP,)),
+            dma((NEP,)),
+            dma((NEP,)),
             dma((NZ,)),
             dma((NZ,)),
             dma((NTP,)),
@@ -627,11 +759,11 @@
             dma((NEP,)),
         ],
         compiler_params=pltpu.CompilerParams(
-            collective_id=0, has_side_effects=True, vmem_limit_bytes=48 * 1024 * 1024
+            collective_id=0, has_side_effects=True, vmem_limit_bytes=67043328
         ),
     )(
         hidden,
-        positions.reshape(ROWS, 1),
+        positions.reshape(1, ROWS),
         ret_state,
         query_weight,
         key_weight,
@@ -644,10 +776,29 @@
         expert_gate,
         expert_up,
         expert_down,
-        route_ids,
-        route_weight,
-        jnp.asarray(constants()),
+        route_ids.T,
+        route_weight.T,
+        table,
     )
+    return pl.pallas_call(
+        state_body,
+        out_shape=(
+            jax.ShapeDtypeStruct((ROWS, COLS), BF16),
+            jax.ShapeDtypeStruct(ret_state.shape, F32),
+        ),
+        in_specs=[anywhere] * 4,
+        out_specs=(anywhere,) * 2,
+        scratch_shapes=[
+            vmem((ROWS, COLS), BF16),
+            vmem((2, ROWS, HEAD), F32),
+            vmem((24, 128), F32),
+            vmem((ROWS, 1, HEAD, HEAD), F32),
+            dma((4,)),
+            dma((GROUPS_OF_ROWS,)),
+            dma((GROUPS_OF_ROWS,)),
+        ],
+        compiler_params=pltpu.CompilerParams(vmem_limit_bytes=67043328),
+    )(updated, parts, table, ret_state)
 
 
 def solution(mesh):

time: 106 us -> 88.1 us (0.83)
  local copies, waits for them, and re-layouts: 17.7 us -> 0 us
    unnamed x28 -> x0, local copies, waits for them, and re-layouts: 16.9 us -> none
    pallas_call x0 -> x1, Pallas kernels: none -> 3.88 us  [per_device(): pl.pallas_call(state_body, out_shape=(jax.ShapeDtypeStruct((ROWS, COLS),...]
    pallas_call x1, Pallas kernels: 86.8 us -> 83.5 us  [per_device(): pl.pallas_call(body, out_shape=(jax.ShapeDtypeStruct((ROWS, COLS), BF16),...]
where the time goes in v2:
time: 88.1 us; the launch traced here: 88 us
  Pallas kernels  87.3 us (99%)
    pallas_call x1, Pallas kernels, per_device(): pl.pallas_call(body, out_shape=(jax.ShapeDtypeStruct((ROWS, COLS), BF16),...  83.5 us
    pallas_call x1, Pallas kernels, per_device(): pl.pallas_call(state_body, out_shape=(jax.ShapeDtypeStruct((ROWS, COLS),...  3.88 us

profile of v2, /device:TPU:1, one launch (start us, length us, event | category | flops | bytes accessed | tf_op | source)
XLA Modules:
  0.0 88.0 jit_solution(1799374510682363468)
XLA Ops:
  0.6 83.5 %shard_map.176 = (bf16[40,256]{1,0:T(8,128)(2,1)}, f32[2,40,128]{2,1,0:T(8,128)}) custom-call(bf16[40,256]{1,0:T(8,128)(2,1)} %hidden.1, s32[1,40]{1,0:T(1,128)} %bitcast.10, f32[40,1,128,128]{3,2,1,0:T(8,128)} %ret_state.3, bf16[256,128]{1,0:T(8,128)(2,1)} %query_weight.1, bf16[256,128]{1,0:T(8,128)(2,1)} %key_weight.1, bf16[256,128]{1,0:T(8,128)(2,1)} %value_weight.1, ...), custom_call_target="tpu_custom_call" | custom-call | tf_op jit(solution)/shard_map/pallas_call | solution.py:700
  84.1 3.9 %shard_map.177 = (bf16[40,256]{1,0:T(8,128)(2,1)}, f32[40,1,128,128]{3,2,1,0:T(8,128)}) custom-call(bf16[40,256]{1,0:T(8,128)(2,1)} %get-tuple-element.4.before, f32[2,40,128]{2,1,0:T(8,128)} %get-tuple-element.5.parts, f32[24,128]{1,0:T(8,128)} %constant.2.clone.table, f32[40,1,128,128]{3,2,1,0:T(8,128)} %ret_state.3), custom_call_target="tpu_custom_call" | custom-call | tf_op jit(solution)/shard_map/pallas_call | solution.py:783

commit v3 on v2

--- a/solution.py
+++ b/solution.py
@@ -88,6 +88,7 @@
     v_table,
     agbuf,
     xbuf,
+    bacc,
     bsend,
     brecv,
     ssout,
@@ -103,6 +104,8 @@
     fsend,
     frecv,
     local_sem,
+    w_send,
+    w_recv,
     a1_send,
     a1_recv,
     a2_send,
@@ -130,6 +133,8 @@
     z = tp // 2
     core = tp % 2
     other = 2 * z + 1 - core
+    down = ep // 4
+    across = ep % 4
 
     mark("load")
     loads = [
@@ -141,10 +146,10 @@
         (head_gain, v_head_gain),
         (mix_gain, v_mix_gain),
         (ffn_gain, v_ffn_gain),
-        (query_weight, v_qkvg.at[:, pl.ds(0, 128)]),
-        (key_weight, v_qkvg.at[:, pl.ds(128, 128)]),
-        (value_weight, v_qkvg.at[:, pl.ds(256, 128)]),
-        (gate_weight, v_qkvg.at[:, pl.ds(384, 128)]),
+        (query_weight, v_qkvg.at[across, :, pl.ds(0, 128)]),
+        (key_weight, v_qkvg.at[across, :, pl.ds(128, 128)]),
+        (value_weight, v_qkvg.at[across, :, pl.ds(256, 128)]),
+        (gate_weight, v_qkvg.at[across, :, pl.ds(384, 128)]),
         (ret_state, v_state),
         (out_weight, v_out),
         (expert_gate, v_gu.at[:, :, pl.ds(0, 128)]),
@@ -175,6 +180,7 @@
         copy.start()
     for copy in copies[:8]:
         copy.wait()
+    agbuf[pl.ds(z, 1)] = v_hidden[...].reshape(1, ROWS, COLS)
 
     mark("prep")
     token = lax.broadcasted_iota(jnp.int32, (ROWS, ROWS), 0)
@@ -213,6 +219,26 @@
             device_id_type=MESH,
         )
 
+    right = 4 * down + (across + 1) % 4
+    left = 4 * down + (across + 3) % 4
+
+    def w_copy(block, half, way, i):
+        part = v_qkvg.at[block, pl.ds(half * 128, 128)]
+        return copy_to(
+            part, part, w_send.at[way, i], w_recv.at[block, half], right if way == 0 else left, tp
+        )
+
+    for copy in copies[8:12]:
+        copy.wait()
+    w_sends = [
+        w_copy(across, 0, 0, 0),
+        w_copy(across, 1, 1, 0),
+        w_copy(across, 1, 0, 1),
+        w_copy(across, 0, 1, 1),
+        w_copy(left % 4, 0, 0, 2),
+        w_copy(right % 4, 1, 1, 2),
+    ]
+
     def a1_copy(i, slot):
         peer = 2 * ((z + ring_offset(i)) % NZ) + core
         return copy_to(v_hidden, agbuf.at[slot], a1_send.at[i], a1_recv.at[slot], ep, peer)
@@ -221,38 +247,54 @@
         a1_copy(NZ - 2 - i, z).start()
         return carry
 
-    mark("a1_issue")
     lax.fori_loop(0, NZ - 1, a1_start, 0)
-
-    def a2_copy(src, row, cc):
+    for copy in w_sends[:4]:
+        copy.start()
+
+    def near(i):
+        return i + (i // 2) * (5 - 2 * i)
+
+    def a2_copy(row, cc):
         return copy_to(
-            src, xbuf.at[ep], a2_send.at[row, cc], a2_recv.at[ep], 2 * row + core, 2 * z + cc
+            agbuf.at[pl.ds(2 * row, 2)],
+            xbuf.at[down, core],
+            a2_send.at[row, cc],
+            a2_recv.at[down, core],
+            4 * row + across,
+            2 * z + cc,
         )
 
-    def a2_from(src, row):
-        target = 2 * row + core
+    def a2_start(i, carry):
+        row = (z // 2 + near(i)) % 4
+        for k in range(2):
+            slot = 2 * row + k
+
+            @pl.when(slot != z)
+            def _():
+                a1_copy(0, slot).wait_recv()
+
         for cc in range(2):
-            mine = (target == ep) & (cc == core)
+            mine = (row == down) & (cc == core)
 
             @pl.when(jnp.logical_not(mine))
             def _():
-                a2_copy(src, row, cc).start()
+                a2_copy(row, cc).start()
 
             @pl.when(mine)
             def _():
-                xbuf[pl.ds(ep, 1)] = src[...].reshape(1, ROWS, COLS)
-
-    agbuf[pl.ds(z, 1)] = v_hidden[...].reshape(1, ROWS, COLS)
-    a2_from(v_hidden, z)
-
-    def a2_start(i, carry):
-        row = (z + ring_offset(i)) % NZ
-        a1_copy(i, row).wait_recv()
-        a2_from(agbuf.at[row], row)
+                xbuf[pl.ds(row, 1), pl.ds(core, 1)] = agbuf[pl.ds(2 * row, 2)].reshape(
+                    1, 1, 2, ROWS, COLS
+                )
+
         return carry
 
     mark("a1_wait_a2_issue")
-    lax.fori_loop(0, NZ - 1, a2_start, 0)
+    lax.fori_loop(0, 4, a2_start, 0)
+    mark("w_forward")
+    w_copy(left % 4, 0, 0, 0).wait_recv()
+    w_sends[4].start()
+    w_copy(right % 4, 1, 1, 0).wait_recv()
+    w_sends[5].start()
 
     mark("ss")
     def square(i, total):
@@ -264,70 +306,70 @@
     ss_copy = copy_to(ssout, ssin, ss_sem.at[0], ss_sem.at[1], ep, other)
     ss_copy.start()
 
-    for copy in copies[8:12]:
-        copy.wait()
-    mix_row = v_mix_gain[:, pl.ds(pl.multiple_of(ep * COLS, COLS), COLS)]
-
     def plane_peer(i):
         down, along = i // 4, i % 4
         down = down + (down // 2) * (5 - 2 * down)
         along = along + (along // 2) * (5 - 2 * along)
         return ((ep // 4 + down) % 4) * 4 + (ep + along) % 4
 
-    def plane_row(i):
-        step = i + (i // 2) * (5 - 2 * i)
-        return (ep // 4 + step) % 4
-
-    def b_copy(slot, peer):
-        return copy_to(bsend.at[peer], brecv.at[slot], b_send.at[peer], b_recv.at[slot], peer, tp)
-
-    def b_rows(i, carry):
-        row = plane_row(i)
-        for k in range(4):
-            peer = 4 * row + k
-
-            @pl.when((peer != ep) | (ep % 2 != core))
+    def b_copy(slot, row):
+        return copy_to(
+            bsend.at[row], brecv.at[slot], b_send.at[row], b_recv.at[slot], 4 * row + across, tp
+        )
+
+    mark("a2_wait")
+    for row in range(4):
+        for parity in range(2):
+
+            @pl.when((row != down) | (parity != core))
             def _():
-                copy_to(
-                    v_hidden, xbuf.at[peer], a2_send.at[0, 0], a2_recv.at[peer], ep, other
-                ).wait_recv()
-
-        rows = xbuf[pl.ds(4 * row, 4)].astype(F32) * mix_row.reshape(1, 1, COLS)
-        rows = rows.reshape(4 * ROWS, COLS).astype(BF16)
-        sums = jnp.dot(rows, v_qkvg[...], preferred_element_type=F32)
-        bsend[pl.ds(4 * row, 4)] = sums.reshape(4, ROWS, 512).astype(BF16)
-        for k in range(4):
-            peer = 4 * row + k
-
-            @pl.when(peer != ep)
-            def _():
-                b_copy(ep, peer).start()
-
-        return carry
+                block = xbuf.at[row, parity]
+                copy_to(block, block, a2_send.at[0, 0], a2_recv.at[row, parity], ep, other).wait_recv()
+
+    def partial(block):
+        at = pl.multiple_of((4 * down + block) * COLS, COLS)
+        gain = v_mix_gain[:, pl.ds(at, COLS)].reshape(1, 1, COLS)
+        rows = xbuf[:, pl.ds(block % 2, 1), pl.ds(block // 2, 1)].reshape(4, ROWS, COLS)
+        rows = (rows.astype(F32) * gain).reshape(4 * ROWS, COLS).astype(BF16)
+        return jnp.dot(
+            rows, v_qkvg[pl.ds(block, 1)].reshape(COLS, 512), preferred_element_type=F32
+        )
 
     mark("b_rows")
-    lax.fori_loop(0, 4, b_rows, 0)
-    brecv[pl.ds(ep, 1)] = bsend[pl.ds(ep, 1)]
+    bacc[...] = partial(across)
+    w_copy(left % 4, 1, 0, 0).wait_recv()
+    bacc[...] += partial(left % 4)
+    w_copy(right % 4, 0, 1, 0).wait_recv()
+    bacc[...] += partial(right % 4)
+    opposite = (across + 2) % 4
+    mark("w_wait")
+    w_copy(opposite, 0, 0, 0).wait_recv()
+    w_copy(opposite, 1, 1, 0).wait_recv()
+    mark("b_last")
+    bsend[...] = (bacc[...] + partial(opposite)).reshape(4, ROWS, 512).astype(BF16)
+
+    def b_start(i, carry):
+        b_copy(down, (down + near(3 - i)) % 4).start()
+        return carry
+
+    lax.fori_loop(0, 3, b_start, 0)
+    brecv[pl.ds(down, 1)] = bsend[pl.ds(down, 1)]
 
     mark("ss_wait")
     ss_copy.wait_recv()
     square_sum = jnp.sum(ssout[...] + ssin[...], axis=-1, keepdims=True)
     factor = lax.rsqrt(square_sum * (1.0 / D) + EPS)
 
-    def b_sum(i, total):
-        row = plane_row(i)
-        for k in range(4):
-            peer = 4 * row + k
-
-            @pl.when(peer != ep)
-            def _():
-                b_copy(peer, peer).wait_recv()
-
-        part = brecv[pl.ds(4 * row, 4)].astype(F32)
-        return total + ((part[0] + part[1]) + (part[2] + part[3]))
-
     mark("b_sum")
-    joined = lax.fori_loop(0, 4, b_sum, jnp.zeros((ROWS, 512), F32))
+
+    def b_wait(i, carry):
+        row = (down + near(i)) % 4
+        b_copy(row, row).wait_recv()
+        return carry
+
+    lax.fori_loop(1, 4, b_wait, 0)
+    part = brecv[...].astype(F32)
+    joined = (part[0] + part[1]) + (part[2] + part[3])
     joined = (joined * factor).astype(BF16).astype(F32)
 
     mark("rot")
@@ -584,22 +626,26 @@
 
     lax.fori_loop(0, NZ - 1, sent_ring, 0)
 
-    def sent_a2(row, carry):
+    for row in range(4):
         for cc in range(2):
 
-            @pl.when((2 * row + core != ep) | (cc != core))
+            @pl.when((row != down) | (cc != core))
             def _():
-                a2_copy(v_hidden, row, cc).wait_send()
-
-        return carry
-
-    lax.fori_loop(0, NZ, sent_a2, 0)
+                a2_copy(row, cc).wait_send()
+
+    for copy in w_sends:
+        copy.wait_send()
+
+    def sent_b(i, carry):
+        b_copy(down, (down + near(i)) % 4).wait_send()
+        return carry
+
+    lax.fori_loop(1, 4, sent_b, 0)
     ss_copy.wait_send()
     d_forward(core, ep).wait_send()
 
     def sent_plane(i, carry):
         peer = (ep + i) % NEP
-        b_copy(ep, peer).wait_send()
         d_copy(peer, ep).wait_send()
         d_forward(core, peer).wait_send()
         return carry
@@ -709,7 +755,7 @@
             vmem((ROWS, COLS), BF16),
             vmem((1, ROWS), jnp.int32),
             vmem((ROWS, 1, HEAD, HEAD), F32),
-            vmem((COLS, 512), BF16),
+            vmem((4, COLS, 512), BF16),
             vmem((1, HEAD), F32),
             vmem((RD, COLS), BF16),
             vmem((1, D), F32),
@@ -720,9 +766,10 @@
             vmem((2, ROWS), F32),
             vmem((24, 128), F32),
             vmem((NZ, ROWS, COLS), BF16),
-            vmem((NEP, ROWS, COLS), BF16),
-            vmem((NEP, ROWS, 512), BF16),
-            vmem((NEP, ROWS, 512), BF16),
+            vmem((4, 2, 2, ROWS, COLS), BF16),
+            vmem((4 * ROWS, 512), F32),
+            vmem((4, ROWS, 512), BF16),
+            vmem((4, ROWS, 512), BF16),
             vmem((ROWS, 128), F32),
             vmem((ROWS, 128), F32),
             vmem((4, ROWS, HEAD), F32),
@@ -736,13 +783,15 @@
             vmem((NEP, 16, 128), BF16),
             vmem((NEP, 16, 128), BF16),
             dma((17,)),
+            dma((2, 3)),
+            dma((4, 2)),
             dma((NZ,)),
             dma((NZ,)),
-            dma((NZ, 2)),
-            dma((NEP,)),
+            dma((4, 2)),
+            dma((4, 2)),
             dma((2,)),
-            dma((NEP,)),
-            dma((NEP,)),
+            dma((4,)),
+            dma((4,)),
             dma((NZ,)),
             dma((NZ,)),
             dma((NTP,)),

time: 88.1 us -> 79.3 us (0.900)
  Pallas kernels: 87.3 us -> 78.5 us
    pallas_call x1, Pallas kernels: 83.5 us -> 74.6 us  [per_device(): pl.pallas_call(body, out_shape=(jax.ShapeDtypeStruct((ROWS, COLS), BF16),...]
where the time goes in v3:
time: 79.3 us; the launch traced here: 79.1 us
  Pallas kernels  78.5 us (99%)
    pallas_call x1, Pallas kernels, per_device(): pl.pallas_call(body, out_shape=(jax.ShapeDtypeStruct((ROWS, COLS), BF16),...  74.6 us
    pallas_call x1, Pallas kernels, per_device(): pl.pallas_call(state_body, out_shape=(jax.ShapeDtypeStruct((ROWS, COLS),...  3.88 us

profile of v3, /device:TPU:1, one launch (start us, length us, event | category | flops | bytes accessed | tf_op | source)
XLA Modules:
  0.0 79.1 jit_solution(17050729475700771525)
XLA Ops:
  0.6 74.6 %shard_map.176 = (bf16[40,256]{1,0:T(8,128)(2,1)}, f32[2,40,128]{2,1,0:T(8,128)}) custom-call(bf16[40,256]{1,0:T(8,128)(2,1)} %hidden.1, s32[1,40]{1,0:T(1,128)} %bitcast.10, f32[40,1,128,128]{3,2,1,0:T(8,128)} %ret_state.3, bf16[256,128]{1,0:T(8,128)(2,1)} %query_weight.1, bf16[256,128]{1,0:T(8,128)(2,1)} %key_weight.1, bf16[256,128]{1,0:T(8,128)(2,1)} %value_weight.1, ...), custom_call_target="tpu_custom_call" | custom-call | tf_op jit(solution)/shard_map/pallas_call | solution.py:746
  75.3 3.9 %shard_map.177 = (bf16[40,256]{1,0:T(8,128)(2,1)}, f32[40,1,128,128]{3,2,1,0:T(8,128)}) custom-call(bf16[40,256]{1,0:T(8,128)(2,1)} %get-tuple-element.4.before, f32[2,40,128]{2,1,0:T(8,128)} %get-tuple-element.5.parts, f32[24,128]{1,0:T(8,128)} %constant.2.clone.table, f32[40,1,128,128]{3,2,1,0:T(8,128)} %ret_state.3), custom_call_target="tpu_custom_call" | custom-call | tf_op jit(solution)/shard_map/pallas_call | solution.py:832

commit v4 on v3

--- a/solution.py
+++ b/solution.py
@@ -21,6 +21,7 @@
 NTP = 16
 NZ = 8
 SLOTS = 128
+LIMIT = 67043328 - 40 * 128 * 128 * 4 - 2 * 16384 * 2
 GROUPS_OF_ROWS = ROWS // 8
 EPS = 1e-06
 
@@ -50,7 +51,7 @@
 
 def ring_offset(i):
     half = i // 2 + 1
-    return half + (i % 2) * (NZ - 2 * half)
+    return half + ((i + 1) % 2) * (NZ - 2 * half)
 
 
 def body(
@@ -72,10 +73,9 @@
     route_weight,
     table,
     updated,
-    state_parts,
+    v_state,
     v_hidden,
     v_pos,
-    v_state,
     v_qkvg,
     v_head_gain,
     v_out,
@@ -98,12 +98,14 @@
     afters,
     psend,
     dbuf,
+    lifted,
     acc_gu,
     ebuf,
     acc_down,
     fsend,
     frecv,
     local_sem,
+    gu_sem,
     w_send,
     w_recv,
     a1_send,
@@ -152,14 +154,34 @@
         (gate_weight, v_qkvg.at[across, :, pl.ds(384, 128)]),
         (ret_state, v_state),
         (out_weight, v_out),
-        (expert_gate, v_gu.at[:, :, pl.ds(0, 128)]),
-        (expert_up, v_gu.at[:, :, pl.ds(128, 128)]),
         (expert_down, v_down),
     ]
     copies = [pltpu.make_async_copy(src, dst, local_sem.at[i]) for i, (src, dst) in enumerate(loads)]
     for copy in copies[:12]:
         copy.start()
 
+    def relative(i):
+        return (z + (i + 1) // 2 * (1 - i % 2 * 2) + NZ) % NZ
+
+    def lift_load(i, up):
+        parity, place = i // NZ, i % NZ
+        source = pl.multiple_of((2 * relative(place) + parity) * COLS, COLS)
+        return pltpu.make_async_copy(
+            (expert_up if up else expert_gate).at[:, pl.ds(source, COLS)],
+            v_gu.at[:, pl.ds(pl.multiple_of(i * COLS, COLS), COLS), pl.ds(128 * up, 128)],
+            gu_sem.at[i, up],
+        )
+
+    def lift_loads(i, carry):
+        lift_load(i, 0).start()
+        lift_load(i, 1).start()
+        return carry
+
+    def lift_loaded(i, carry):
+        lift_load(i, 0).wait()
+        lift_load(i, 1).wait()
+        return carry
+
     barrier = pltpu.get_barrier_semaphore()
 
     def greet_plane(i, carry):
@@ -178,6 +200,7 @@
     pl.semaphore_signal(barrier, inc=1, device_id=(ep, other), device_id_type=MESH)
     for copy in copies[12:]:
         copy.start()
+    lax.fori_loop(0, NTP, lift_loads, 0)
     for copy in copies[:8]:
         copy.wait()
     agbuf[pl.ds(z, 1)] = v_hidden[...].reshape(1, ROWS, COLS)
@@ -306,11 +329,12 @@
     ss_copy = copy_to(ssout, ssin, ss_sem.at[0], ss_sem.at[1], ep, other)
     ss_copy.start()
 
-    def plane_peer(i):
-        down, along = i // 4, i % 4
-        down = down + (down // 2) * (5 - 2 * down)
-        along = along + (along // 2) * (5 - 2 * along)
-        return ((ep // 4 + down) % 4) * 4 + (ep + along) % 4
+    steps = (0, 1, 3, 2)
+    plane = [
+        4 * lax.rem(down + row, 4) + lax.rem(across + column_step, 4)
+        for row in steps
+        for column_step in steps
+    ]
 
     def b_copy(slot, row):
         return copy_to(
@@ -384,8 +408,6 @@
     readbuf[0] = rotated_query
     readbuf[1] = rotated_key
     readbuf[2] = value
-    state_parts[0] = rotated_key
-    state_parts[1] = value
     mark("retain")
     copies[12].wait()
 
@@ -399,6 +421,7 @@
             state = (
                 decay * v_state[8 * group + k, 0] + key_columns[:, k : k + 1] * values[k : k + 1, :]
             )
+            v_state[8 * group + k, 0] = state
             reads.append(jnp.sum(query_columns[:, k : k + 1] * state, axis=0, keepdims=True))
         readbuf[3, at, :] = jnp.concatenate(reads, axis=0)
         return carry
@@ -422,7 +445,7 @@
             )
 
         def begin(i, carry):
-            direct(NZ - 2 - i, tp).start()
+            direct(i, tp).start()
             return carry
 
         lax.fori_loop(0, NZ - 1, begin, 0)
@@ -487,7 +510,7 @@
         return copy_to(afters.at[z], afters.at[slot], g_send.at[i], g_recv.at[slot], ep, peer)
 
     def g_start(i, carry):
-        g_copy(NZ - 2 - i, z).start()
+        g_copy(i, z).start()
         return carry
 
     lax.fori_loop(0, NZ - 1, g_start, 0)
@@ -502,82 +525,95 @@
 
     placing = placed.astype(BF16)
 
-    def pack(row):
+    def pack(half, k):
         packed = lax.dot_general(
             placing,
-            afters[pl.ds(row, 1)].reshape(ROWS, COLS),
+            afters[pl.ds(relative(4 * half + k), 1)].reshape(ROWS, COLS),
             (((0,), (0,)), ((), ())),
             preferred_element_type=F32,
         )
-        psend[:, pl.ds(row, 1)] = halves_below(packed).astype(BF16).reshape(NEP, 1, 16, 128)
-
-    pack(z)
-
-    def pack_next(i, carry):
-        row = (z + ring_offset(i)) % NZ
-        g_copy(i, row).wait_recv()
-        pack(row)
-        return carry
-
-    mark("after_gather")
-    lax.fori_loop(0, NZ - 1, pack_next, 0)
-
-    def d_copy(peer, source):
+        packed = halves_below(packed).astype(BF16)
+        psend[half, :, pl.ds(k, 1)] = packed.reshape(NEP, 1, 16, 128)
+
+    def d_copy(half, peer, source):
         return copy_to(
-            psend.at[peer], dbuf.at[core, source], d_send.at[peer], d_recv.at[source], peer, tp
-        )
-
-    def d_forward(parity, source):
-        block = dbuf.at[parity, source]
-        return copy_to(block, block, d_fwd.at[source], d_other.at[source], ep, other)
-
-    def d_start(i, carry):
-        d_copy(plane_peer(NEP - 1 - i), ep).start()
-        return carry
-
-    mark("d_issue")
-    lax.fori_loop(0, NEP - 1, d_start, 0)
-    dbuf[pl.ds(core, 1), pl.ds(ep, 1)] = psend[pl.ds(ep, 1)].reshape(1, 1, NZ, 16, 128)
-    d_forward(core, ep).start()
-
-    def d_arrive(i, carry):
-        peer = plane_peer(i)
-        d_copy(peer, peer).wait_recv()
-        d_forward(core, peer).start()
-        return carry
-
+            psend.at[half, peer],
+            dbuf.at[core, half, source],
+            d_send.at[half, peer],
+            d_recv.at[half, source],
+            peer,
+            tp,
+        )
+
+    def d_forward(half, parity, source):
+        block = dbuf.at[parity, half, source]
+        return copy_to(block, block, d_fwd.at[half, source], d_other.at[half, source], ep, other)
+
+    def pack_next(half):
+        def one(k, carry):
+            g_copy(4 * half + k - 1, relative(4 * half + k)).wait_recv()
+            pack(half, k)
+            return carry
+
+        return one
+
+    pack(0, 0)
     acc_gu[...] = jnp.zeros_like(acc_gu)
-    mark("d_wait")
-    lax.fori_loop(1, NEP, d_arrive, 0)
-    copies[14].wait()
-    copies[15].wait()
+    for half in range(2):
+        mark(f"after_gather{half}")
+        lax.fori_loop(1 - half, 4, pack_next(half), 0)
+        mark(f"d_issue{half}")
+        for peer in plane[:0:-1]:
+            d_copy(half, peer, ep).start()
+        dbuf[pl.ds(core, 1), half, pl.ds(ep, 1)] = psend[half, pl.ds(ep, 1)].reshape(
+            1, 1, 4, 16, 128
+        )
+        d_forward(half, core, ep).start()
+
+    def d_arrive(half):
+        for peer in plane[1:]:
+            d_copy(half, peer, peer).wait_recv()
+            d_forward(half, core, peer).start()
+
+    def d_other_wait(half):
+        def one(source, carry):
+            d_forward(half, 1 - core, source).wait_recv()
+            return carry
+
+        return one
+
     square_of = acc_gu.at[2]
 
-    def lift(parity):
-        def one(row, carry):
-            at = pl.multiple_of((2 * row + parity) * COLS, COLS)
-            block = dbuf[pl.ds(parity, 1), :, pl.ds(row, 1)].reshape(NEP, 16, 128)
+    def lift(half, parity):
+        for k in range(4):
+            at = pl.multiple_of((2 * relative(4 * half + k) + parity) * COLS, COLS)
+            block = dbuf[pl.ds(parity, 1), half, :, k].reshape(NEP, 16, 128)
             low, high = halves_beside(block)
             square_of[:, :128] += low * low + high * high
             both = jnp.concatenate([low, high], axis=1) * v_ffn_gain[:, pl.ds(at, COLS)]
-            both = both.astype(BF16)
-            for j in range(2):
-                acc_gu[j] += jnp.dot(both, v_gu[j, pl.ds(at, COLS), :], preferred_element_type=F32)
-            return carry
-
-        lax.fori_loop(0, NZ, one, 0)
-
-    mark("lift_own")
-    lift(core)
-
-    def d_other_wait(source, carry):
-        d_forward(1 - core, source).wait_recv()
-        return carry
-
+            lifted[:, k * COLS : (k + 1) * COLS] = both.astype(BF16)
+        at = pl.multiple_of((parity * NZ + 4 * half) * COLS, 4 * COLS)
+        for j in range(2):
+            acc_gu[j] += jnp.dot(
+                lifted[...], v_gu[j, pl.ds(at, 4 * COLS), :], preferred_element_type=F32
+            )
+
+    mark("d_wait0")
+    d_arrive(0)
+    lax.fori_loop(0, NTP, lift_loaded, 0)
+    mark("lift_own0")
+    lift(0, core)
+    mark("d_wait1")
+    d_arrive(1)
+    lax.fori_loop(0, NEP, d_other_wait(0), 0)
+    mark("lift_other0")
+    lift(0, 1 - core)
+    mark("lift_own1")
+    lift(1, core)
     mark("lift_wait")
-    lax.fori_loop(0, NEP, d_other_wait, 0)
-    mark("lift_other")
-    lift(1 - core)
+    lax.fori_loop(0, NEP, d_other_wait(1), 0)
+    mark("lift_other1")
+    lift(1, 1 - core)
     mark("act")
     inner = lax.rsqrt(
         jnp.sum(square_of[:, :128], axis=-1, keepdims=True) * (1.0 / D) + EPS
@@ -586,7 +622,7 @@
     chosen = jnp.where(own_expert, acc_gu[0], acc_gu[1]) * inner
     activated = jax.nn.silu(chosen[:, :128]) * chosen[:, 128:]
     ebuf[pl.ds(tp, 1)] = activated.astype(BF16).reshape(1, SLOTS, 128)
-    copies[16].wait()
+    copies[14].wait()
 
     def lower(row, first_step):
         @pl.when(first_step)
@@ -611,11 +647,8 @@
             fsend.at[peer], frecv.at[source], f_send.at[peer], f_recv.at[source], peer, tp
         )
 
-    def f_start(i, carry):
-        f_copy((ep + i) % NEP, ep).start()
-        return carry
-
-    lax.fori_loop(1, NEP, f_start, 0)
+    for peer in plane[:0:-1]:
+        f_copy(peer, ep).start()
     frecv[pl.ds(ep, 1)] = fsend[pl.ds(ep, 1)]
 
     mark("sent")
@@ -642,12 +675,14 @@
 
     lax.fori_loop(1, 4, sent_b, 0)
     ss_copy.wait_send()
-    d_forward(core, ep).wait_send()
+    for half in range(2):
+        d_forward(half, core, ep).wait_send()
 
     def sent_plane(i, carry):
         peer = (ep + i) % NEP
-        d_copy(peer, ep).wait_send()
-        d_forward(core, peer).wait_send()
+        for half in range(2):
+            d_copy(half, peer, ep).wait_send()
+            d_forward(half, core, peer).wait_send()
         return carry
 
     lax.fori_loop(1, NEP, sent_plane, 0)
@@ -676,49 +711,15 @@
     mark("")
 
 
-def state_body(
-    before, parts, table, ret_state, updated, next_state, v_updated, v_parts, v_table, v_state, sem, load, store
-):
+def state_body(before, state, updated, next_state, sem):
     copies = [
-        pltpu.make_async_copy(parts, v_parts, sem.at[0]),
-        pltpu.make_async_copy(table, v_table, sem.at[1]),
-        pltpu.make_async_copy(before, v_updated, sem.at[2]),
+        pltpu.make_async_copy(before, updated, sem.at[0]),
+        pltpu.make_async_copy(state, next_state, sem.at[1]),
     ]
-    out = pltpu.make_async_copy(v_updated, updated, sem.at[3])
-
-    def rows_in(group):
-        at = pl.ds(8 * group, 8)
-        return pltpu.make_async_copy(ret_state.at[at], v_state.at[at], load.at[group])
-
-    def rows_out(group):
-        at = pl.ds(8 * group, 8)
-        return pltpu.make_async_copy(v_state.at[at], next_state.at[at], store.at[group])
-
     for copy in copies:
         copy.start()
-    for group in range(GROUPS_OF_ROWS):
-        rows_in(group).start()
     for copy in copies:
         copy.wait()
-    out.start()
-    decay = v_table[pl.ds(lax.axis_index("tp"), 1), :]
-
-    def one(group, carry):
-        at = pl.ds(pl.multiple_of(8 * group, 8), 8)
-        key_columns = v_parts[0, at, :].T
-        values = v_parts[1, at, :]
-        rows_in(group).wait()
-        for k in range(8):
-            v_state[8 * group + k, 0] = (
-                decay * v_state[8 * group + k, 0] + key_columns[:, k : k + 1] * values[k : k + 1, :]
-            )
-        rows_out(group).start()
-        return carry
-
-    lax.fori_loop(0, GROUPS_OF_ROWS, one, 0)
-    out.wait()
-    for group in range(GROUPS_OF_ROWS):
-        rows_out(group).wait()
 
 
 def per_device(
@@ -746,15 +747,14 @@
     updated, parts = pl.pallas_call(
         body,
         out_shape=(
-            jax.ShapeDtypeStruct((ROWS, COLS), BF16),
-            jax.ShapeDtypeStruct((2, ROWS, HEAD), F32),
+            pltpu.VMEM((ROWS, COLS), BF16),
+            pltpu.VMEM(ret_state.shape, F32),
         ),
         in_specs=[anywhere] * 17,
         out_specs=(pl.BlockSpec(memory_space=pltpu.VMEM),) * 2,
         scratch_shapes=[
             vmem((ROWS, COLS), BF16),
             vmem((1, ROWS), jnp.int32),
-            vmem((ROWS, 1, HEAD, HEAD), F32),
             vmem((4, COLS, 512), BF16),
             vmem((1, HEAD), F32),
             vmem((RD, COLS), BF16),
@@ -775,14 +775,16 @@
             vmem((4, ROWS, HEAD), F32),
             vmem((NTP, ROWS, HEAD), BF16),
             vmem((NZ, ROWS, COLS), BF16),
-            vmem((NEP, NZ, 16, 128), BF16),
-            vmem((2, NEP, NZ, 16, 128), BF16),
+            vmem((2, NEP, 4, 16, 128), BF16),
+            vmem((2, 2, NEP, 4, 16, 128), BF16),
+            vmem((SLOTS, 4 * COLS), BF16),
             vmem((3, SLOTS, COLS), F32),
             vmem((NTP, SLOTS, 128), BF16),
             vmem((2, SLOTS, COLS), F32),
             vmem((NEP, 16, 128), BF16),
             vmem((NEP, 16, 128), BF16),
-            dma((17,)),
+            dma((15,)),
+            dma((NTP, 2)),
             dma((2, 3)),
             dma((4, 2)),
             dma((NZ,)),
@@ -797,10 +799,10 @@
             dma((NTP,)),
             dma((NZ,)),
             dma((NZ,)),
-            dma((NEP,)),
-            dma((NEP,)),
-            dma((NEP,)),
-            dma((NEP,)),
+            dma((2, NEP)),
+            dma((2, NEP)),
+            dma((2, NEP)),
+            dma((2, NEP)),
             dma((NZ,)),
             dma((NZ,)),
             dma((NTP,)),
@@ -808,7 +810,7 @@
             dma((NEP,)),
         ],
         compiler_params=pltpu.CompilerParams(
-            collective_id=0, has_side_effects=True, vmem_limit_bytes=67043328
+            collective_id=0, has_side_effects=True, vmem_limit_bytes=LIMIT
         ),
     )(
         hidden,
@@ -835,19 +837,11 @@
             jax.ShapeDtypeStruct((ROWS, COLS), BF16),
             jax.ShapeDtypeStruct(ret_state.shape, F32),
         ),
-        in_specs=[anywhere] * 4,
+        in_specs=[pl.BlockSpec(memory_space=pl.ANY)] * 2,
         out_specs=(anywhere,) * 2,
-        scratch_shapes=[
-            vmem((ROWS, COLS), BF16),
-            vmem((2, ROWS, HEAD), F32),
-            vmem((24, 128), F32),
-            vmem((ROWS, 1, HEAD, HEAD), F32),
-            dma((4,)),
-            dma((GROUPS_OF_ROWS,)),
-            dma((GROUPS_OF_ROWS,)),
-        ],
-        compiler_params=pltpu.CompilerParams(vmem_limit_bytes=67043328),
-    )(updated, parts, table, ret_state)
+        scratch_shapes=[dma((2,))],
+        compiler_params=pltpu.CompilerParams(vmem_limit_bytes=1024 * 1024),
+    )(updated, parts)
 
 
 def solution(mesh):

time: 79.3 us -> 71.7 us (0.904)
  Pallas kernels: 78.5 us -> 71 us
    pallas_call x1, Pallas kernels: 74.6 us -> 69.5 us  [per_device(): pl.pallas_call(body, out_shape=(pltpu.VMEM((ROWS, COLS), BF16), pltpu.VME...]
    pallas_call x1, Pallas kernels: 3.88 us -> 1.52 us  [per_device(): pl.pallas_call(state_body, out_shape=(jax.ShapeDtypeStruct((ROWS, COLS),...]
where the time goes in v4:
time: 71.7 us; the launch traced here: 71.6 us
  Pallas kernels  71 us (99%)
    pallas_call x1, Pallas kernels, per_device(): pl.pallas_call(body, out_shape=(pltpu.VMEM((ROWS, COLS), BF16), pltpu.VME...  69.5 us
    pallas_call x1, Pallas kernels, per_device(): pl.pallas_call(state_body, out_shape=(jax.ShapeDtypeStruct((ROWS, COLS),...  1.52 us

profile of v4, /device:TPU:1, one launch (start us, length us, event | category | flops | bytes accessed | tf_op | source)
XLA Modules:
  0.0 71.6 jit_solution(9576291304255262682)
XLA Ops:
  0.6 69.5 %shard_map.176 = (bf16[40,256]{1,0:T(8,128)(2,1)S(1)}, f32[40,1,128,128]{3,2,1,0:T(8,128)S(1)}) custom-call(bf16[40,256]{1,0:T(8,128)(2,1)} %hidden.1, s32[1,40]{1,0:T(1,128)} %bitcast.10, f32[40,1,128,128]{3,2,1,0:T(8,128)} %ret_state.1, bf16[256,128]{1,0:T(8,128)(2,1)} %query_weight.1, bf16[256,128]{1,0:T(8,128)(2,1)} %key_weight.1, ...), custom_call_target="tpu_custom_call" | custom-call | tf_op jit(solution)/shard_map/pallas_call | solution.py:747
  70.1 1.5 %shard_map.177 = (bf16[40,256]{1,0:T(8,128)(2,1)}, f32[40,1,128,128]{3,2,1,0:T(8,128)}) custom-call(bf16[40,256]{1,0:T(8,128)(2,1)S(1)} %get-tuple-element.4.before, f32[40,1,128,128]{3,2,1,0:T(8,128)S(1)} %get-tuple-element.5.state), custom_call_target="tpu_custom_call" | custom-call | tf_op jit(solution)/shard_map/pallas_call | solution.py:834

commit v5 on v4

--- a/solution.py
+++ b/solution.py
@@ -94,6 +94,7 @@
     ssout,
     ssin,
     readbuf,
+    spread,
     cbuf,
     afters,
     psend,
@@ -411,18 +412,35 @@
     mark("retain")
     copies[12].wait()
 
+    own_block = (
+        lax.rem(lax.broadcasted_iota(jnp.int32, (32, 8 * HEAD), 0), 8)
+        == lax.broadcasted_iota(jnp.int32, (32, 8 * HEAD), 1) // HEAD
+    )
+    spread[...] = jnp.where(own_block, 1.0, 0.0).astype(BF16)
+
+    def terms(rows):
+        high = rows.astype(BF16).astype(F32)
+        middle = (rows - high).astype(BF16).astype(F32)
+        low = rows - high - middle
+        return jnp.concatenate([high, middle, low, jnp.zeros_like(rows)], axis=0).astype(BF16)
+
+    def over_rows(stack, columns):
+        return lax.dot_general(
+            stack, columns, (((0,), (0,)), ((), ())), preferred_element_type=F32
+        )
+
     def retain(group, carry):
         at = pl.ds(pl.multiple_of(8 * group, 8), 8)
-        query_columns = readbuf[0, at, :].T
-        key_columns = readbuf[1, at, :].T
-        values = readbuf[2, at, :]
+        values = jnp.concatenate([readbuf[2, at, :]] * 4, axis=0)
+        values = jnp.where(own_block, jnp.concatenate([values] * 8, axis=1), 0.0).astype(BF16)
+        outer = over_rows(terms(readbuf[1, at, :]), values)
+        query = over_rows(terms(readbuf[0, at, :]), spread[...])
         reads = []
         for k in range(8):
-            state = (
-                decay * v_state[8 * group + k, 0] + key_columns[:, k : k + 1] * values[k : k + 1, :]
-            )
+            block = slice(k * HEAD, (k + 1) * HEAD)
+            state = decay * v_state[8 * group + k, 0] + outer[:, block]
             v_state[8 * group + k, 0] = state
-            reads.append(jnp.sum(query_columns[:, k : k + 1] * state, axis=0, keepdims=True))
+            reads.append(jnp.sum(query[:, block] * state, axis=0, keepdims=True))
         readbuf[3, at, :] = jnp.concatenate(reads, axis=0)
         return carry
 
@@ -434,7 +452,7 @@
     mixed = normal * v_head_gain[...] * jax.nn.silu(gate_rows)
     cbuf[pl.ds(tp, 1)] = mixed.astype(BF16).reshape(1, ROWS, HEAD)
 
-    def gather(buf, send_sem, fwd_sem, recv_sem, consume):
+    def gather(buf, send_sem, fwd_sem, recv_sem, consume, both=False, lag=0):
         def direct(i, slot):
             peer = 2 * ((z + ring_offset(i)) % NZ) + core
             return copy_to(buf.at[slot], buf.at[slot], send_sem.at[i], recv_sem.at[slot], ep, peer)
@@ -444,35 +462,48 @@
                 buf.at[slot], buf.at[slot], fwd_sem.at[row], recv_sem.at[slot], ep, other
             )
 
+        def cross(i, slot):
+            peer = 2 * lax.rem(z + ring_offset(i), NZ) + 1 - core
+            return copy_to(
+                buf.at[slot], buf.at[slot], fwd_sem.at[i], recv_sem.at[slot], ep, peer
+            )
+
         def begin(i, carry):
             direct(i, tp).start()
+            if both:
+                cross(i, tp).start()
             return carry
 
         lax.fori_loop(0, NZ - 1, begin, 0)
-        forward(z, tp).start()
+        forward(NZ - 1 if both else z, tp).start()
 
         def step(i, carry):
             @pl.when(i < NZ - 1)
             def _():
                 row = (z + ring_offset(i)) % NZ
                 direct(0, 2 * row + core).wait_recv()
-                forward(row, 2 * row + core).start()
-
-            before = lax.select(i > 0, (z + ring_offset(lax.max(i - 1, 0))) % NZ, z)
-            forward(before, 2 * before + 1 - core).wait_recv()
-            consume(before, i == 0)
+                if not both:
+                    forward(row, 2 * row + core).start()
+
+            @pl.when(i >= lag)
+            def _():
+                place = i - lag
+                before = relative(place)
+                forward(before, 2 * before + 1 - core).wait_recv()
+                consume(before, place == 0)
+
             return carry
 
-        lax.fori_loop(0, NZ, step, 0)
+        lax.fori_loop(0, NZ + lag, step, 0)
 
         def finish():
             def one(i, carry):
                 direct(i, tp).wait_send()
-                forward((z + ring_offset(i)) % NZ, tp).wait_send()
+                forward(i if both else (z + ring_offset(i)) % NZ, tp).wait_send()
                 return carry
 
             lax.fori_loop(0, NZ - 1, one, 0)
-            forward(z, tp).wait_send()
+            forward(NZ - 1 if both else z, tp).wait_send()
 
         return finish
 
@@ -499,7 +530,7 @@
             projected[1] += part[:, 128:]
 
     mark("c_gather")
-    finish_c = gather(cbuf, c_send, c_fwd, c_recv, project)
+    finish_c = gather(cbuf, c_send, c_fwd, c_recv, project, both=True)
     mark("after_pack")
     own = v_hidden[...].astype(F32)
     after = (own + jnp.concatenate([projected[0], projected[1]], axis=1)).astype(BF16)
@@ -636,7 +667,7 @@
             acc_down[j] += jnp.dot(both, v_down[j, pl.ds(at, COLS), :], preferred_element_type=F32)
 
     mark("e_gather")
-    finish_e = gather(ebuf, e_send, e_fwd, e_recv, lower)
+    finish_e = gather(ebuf, e_send, e_fwd, e_recv, lower, lag=1)
     mark("result")
     result = jnp.where(own_expert, acc_down[0], acc_down[1])
 
@@ -773,6 +804,7 @@
             vmem((ROWS, 128), F32),
             vmem((ROWS, 128), F32),
             vmem((4, ROWS, HEAD), F32),
+            vmem((32, 8 * HEAD), BF16),
             vmem((NTP, ROWS, HEAD), BF16),
             vmem((NZ, ROWS, COLS), BF16),
             vmem((2, NEP, 4, 16, 128), BF16),

time: 71.7 us -> 70 us (0.976)
  Pallas kernels: 71 us -> 69.3 us
    pallas_call x1, Pallas kernels: 69.5 us -> 67.8 us  [per_device(): pl.pallas_call(body, out_shape=(pltpu.VMEM((ROWS, COLS), BF16), pltpu.VME...]
where the time goes in v5:
time: 70 us
  Pallas kernels  69.3 us (99%)
    pallas_call x1, Pallas kernels, per_device(): pl.pallas_call(body, out_shape=(pltpu.VMEM((ROWS, COLS), BF16), pltpu.VME...  67.8 us
    pallas_call x1, Pallas kernels, per_device(): pl.pallas_call(state_body, out_shape=(jax.ShapeDtypeStruct((ROWS, COLS),...  1.52 us

profile of v5, /device:TPU:1, one launch (start us, length us, event | category | flops | bytes accessed | tf_op | source)
XLA Modules:
  0.0 70.0 jit_solution(11408350253179032558)
XLA Ops:
  0.6 67.8 %shard_map.176 = (bf16[40,256]{1,0:T(8,128)(2,1)S(1)}, f32[40,1,128,128]{3,2,1,0:T(8,128)S(1)}) custom-call(bf16[40,256]{1,0:T(8,128)(2,1)} %hidden.1, s32[1,40]{1,0:T(1,128)} %bitcast.10, f32[40,1,128,128]{3,2,1,0:T(8,128)} %ret_state.1, bf16[256,128]{1,0:T(8,128)(2,1)} %query_weight.1, bf16[256,128]{1,0:T(8,128)(2,1)} %key_weight.1, ...), custom_call_target="tpu_custom_call" | custom-call | tf_op jit(solution)/shard_map/pallas_call | solution.py:778
  68.4 1.5 %shard_map.177 = (bf16[40,256]{1,0:T(8,128)(2,1)}, f32[40,1,128,128]{3,2,1,0:T(8,128)}) custom-call(bf16[40,256]{1,0:T(8,128)(2,1)S(1)} %get-tuple-element.4.before, f32[40,1,128,128]{3,2,1,0:T(8,128)S(1)} %get-tuple-element.5.state), custom_call_target="tpu_custom_call" | custom-call | tf_op jit(solution)/shard_map/pallas_call | solution.py:866

commit v6 on v5

--- a/solution.py
+++ b/solution.py
@@ -21,6 +21,8 @@
 NTP = 16
 NZ = 8
 SLOTS = 128
+MESSAGES = 2
+PER = NZ // MESSAGES
 LIMIT = 67043328 - 40 * 128 * 128 * 4 - 2 * 16384 * 2
 GROUPS_OF_ROWS = ROWS // 8
 EPS = 1e-06
@@ -95,6 +97,7 @@
     ssin,
     readbuf,
     spread,
+    combine_terms,
     cbuf,
     afters,
     psend,
@@ -229,6 +232,17 @@
     ranks = jnp.dot(earlier, named.astype(BF16), preferred_element_type=F32)
     placed = jnp.where(ranks == (lane % 4).astype(F32), named, 0.0)
     combine = placed * jnp.where(first, column(v_weight[0:1, :]), column(v_weight[1:2, :]))
+    high = combine.astype(BF16).astype(F32)
+    middle = (combine - high).astype(BF16).astype(F32)
+    combine_terms[...] = jnp.concatenate(
+        [high, middle, combine - high - middle, jnp.zeros((8, 128), F32)], axis=0
+    ).astype(BF16)
+
+    own_block = (
+        lax.rem(lax.broadcasted_iota(jnp.int32, (32, 8 * HEAD), 0), 8)
+        == lax.broadcasted_iota(jnp.int32, (32, 8 * HEAD), 1) // HEAD
+    )
+    spread[...] = jnp.where(own_block, 1.0, 0.0).astype(BF16)
 
     mark("barrier")
     pl.semaphore_wait(barrier, 2 * (NEP - 1) + (NZ - 1) + 1)
@@ -333,8 +347,10 @@
     steps = (0, 1, 3, 2)
     plane = [
         4 * lax.rem(down + row, 4) + lax.rem(across + column_step, 4)
-        for row in steps
-        for column_step in steps
+        for row, column_step in sorted(
+            ((row, column_step) for row in range(4) for column_step in range(4)),
+            key=lambda step: min(step[0], 4 - step[0]) + min(step[1], 4 - step[1]),
+        )
     ]
 
     def b_copy(slot, row):
@@ -411,12 +427,6 @@
     readbuf[2] = value
     mark("retain")
     copies[12].wait()
-
-    own_block = (
-        lax.rem(lax.broadcasted_iota(jnp.int32, (32, 8 * HEAD), 0), 8)
-        == lax.broadcasted_iota(jnp.int32, (32, 8 * HEAD), 1) // HEAD
-    )
-    spread[...] = jnp.where(own_block, 1.0, 0.0).astype(BF16)
 
     def terms(rows):
         high = rows.astype(BF16).astype(F32)
@@ -444,7 +454,8 @@
         readbuf[3, at, :] = jnp.concatenate(reads, axis=0)
         return carry
 
-    lax.fori_loop(0, ROWS // 8, retain, 0)
+    for group in range(ROWS // 8):
+        retain(group, 0)
     mark("groupnorm")
     read = readbuf[3]
     centered = read - jnp.mean(read, axis=-1, keepdims=True)
@@ -530,7 +541,7 @@
             projected[1] += part[:, 128:]
 
     mark("c_gather")
-    finish_c = gather(cbuf, c_send, c_fwd, c_recv, project, both=True)
+    finish_c = gather(cbuf, c_send, c_fwd, c_recv, project, lag=1)
     mark("after_pack")
     own = v_hidden[...].astype(F32)
     after = (own + jnp.concatenate([projected[0], projected[1]], axis=1)).astype(BF16)
@@ -559,7 +570,7 @@
     def pack(half, k):
         packed = lax.dot_general(
             placing,
-            afters[pl.ds(relative(4 * half + k), 1)].reshape(ROWS, COLS),
+            afters[pl.ds(relative(PER * half + k), 1)].reshape(ROWS, COLS),
             (((0,), (0,)), ((), ())),
             preferred_element_type=F32,
         )
@@ -582,7 +593,7 @@
 
     def pack_next(half):
         def one(k, carry):
-            g_copy(4 * half + k - 1, relative(4 * half + k)).wait_recv()
+            g_copy(PER * half + k - 1, relative(PER * half + k)).wait_recv()
             pack(half, k)
             return carry
 
@@ -590,14 +601,14 @@
 
     pack(0, 0)
     acc_gu[...] = jnp.zeros_like(acc_gu)
-    for half in range(2):
+    for half in range(MESSAGES):
         mark(f"after_gather{half}")
-        lax.fori_loop(1 - half, 4, pack_next(half), 0)
+        lax.fori_loop(0 if half else 1, PER, pack_next(half), 0)
         mark(f"d_issue{half}")
         for peer in plane[:0:-1]:
             d_copy(half, peer, ep).start()
         dbuf[pl.ds(core, 1), half, pl.ds(ep, 1)] = psend[half, pl.ds(ep, 1)].reshape(
-            1, 1, 4, 16, 128
+            1, 1, PER, 16, 128
         )
         d_forward(half, core, ep).start()
 
@@ -616,35 +627,34 @@
     square_of = acc_gu.at[2]
 
     def lift(half, parity):
-        for k in range(4):
-            at = pl.multiple_of((2 * relative(4 * half + k) + parity) * COLS, COLS)
+        for k in range(PER):
+            at = pl.multiple_of((2 * relative(PER * half + k) + parity) * COLS, COLS)
             block = dbuf[pl.ds(parity, 1), half, :, k].reshape(NEP, 16, 128)
             low, high = halves_beside(block)
             square_of[:, :128] += low * low + high * high
             both = jnp.concatenate([low, high], axis=1) * v_ffn_gain[:, pl.ds(at, COLS)]
             lifted[:, k * COLS : (k + 1) * COLS] = both.astype(BF16)
-        at = pl.multiple_of((parity * NZ + 4 * half) * COLS, 4 * COLS)
+        at = pl.multiple_of((parity * NZ + PER * half) * COLS, PER * COLS)
         for j in range(2):
             acc_gu[j] += jnp.dot(
-                lifted[...], v_gu[j, pl.ds(at, 4 * COLS), :], preferred_element_type=F32
+                lifted[...], v_gu[j, pl.ds(at, PER * COLS), :], preferred_element_type=F32
             )
 
-    mark("d_wait0")
-    d_arrive(0)
-    lax.fori_loop(0, NTP, lift_loaded, 0)
-    mark("lift_own0")
-    lift(0, core)
-    mark("d_wait1")
-    d_arrive(1)
-    lax.fori_loop(0, NEP, d_other_wait(0), 0)
-    mark("lift_other0")
-    lift(0, 1 - core)
-    mark("lift_own1")
-    lift(1, core)
+    for half in range(MESSAGES):
+        mark(f"d_wait{half}")
+        d_arrive(half)
+        if half == 0:
+            lax.fori_loop(0, NTP, lift_loaded, 0)
+        else:
+            lax.fori_loop(0, NEP, d_other_wait(half - 1), 0)
+            mark(f"lift_other{half - 1}")
+            lift(half - 1, 1 - core)
+        mark(f"lift_own{half}")
+        lift(half, core)
     mark("lift_wait")
-    lax.fori_loop(0, NEP, d_other_wait(1), 0)
-    mark("lift_other1")
-    lift(1, 1 - core)
+    lax.fori_loop(0, NEP, d_other_wait(MESSAGES - 1), 0)
+    mark("lift_last")
+    lift(MESSAGES - 1, 1 - core)
     mark("act")
     inner = lax.rsqrt(
         jnp.sum(square_of[:, :128], axis=-1, keepdims=True) * (1.0 / D) + EPS
@@ -706,12 +716,12 @@
 
     lax.fori_loop(1, 4, sent_b, 0)
     ss_copy.wait_send()
-    for half in range(2):
+    for half in range(MESSAGES):
         d_forward(half, core, ep).wait_send()
 
     def sent_plane(i, carry):
         peer = (ep + i) % NEP
-        for half in range(2):
+        for half in range(MESSAGES):
             d_copy(half, peer, ep).wait_send()
             d_forward(half, core, peer).wait_send()
         return carry
@@ -729,9 +739,8 @@
     lax.fori_loop(1, NEP, f_wait, 0)
     mark("combine")
     back = jnp.concatenate(halves_beside(frecv[...]), axis=1)
-    weighted = jnp.dot(
-        combine, back, preferred_element_type=F32, precision=lax.Precision.HIGHEST
-    )
+    weighted = jnp.dot(combine_terms[...], back.astype(BF16), preferred_element_type=F32)
+    weighted = weighted[:ROWS] + weighted[ROWS : 2 * ROWS] + weighted[2 * ROWS : 3 * ROWS]
     updated[...] = (after.astype(F32) + weighted).astype(BF16)
 
     def f_sent(i, carry):
@@ -805,11 +814,12 @@
             vmem((ROWS, 128), F32),
             vmem((4, ROWS, HEAD), F32),
             vmem((32, 8 * HEAD), BF16),
+            vmem((128, 128), BF16),
             vmem((NTP, ROWS, HEAD), BF16),
             vmem((NZ, ROWS, COLS), BF16),
-            vmem((2, NEP, 4, 16, 128), BF16),
-            vmem((2, 2, NEP, 4, 16, 128), BF16),
-            vmem((SLOTS, 4 * COLS), BF16),
+            vmem((MESSAGES, NEP, PER, 16, 128), BF16),
+            vmem((2, MESSAGES, NEP, PER, 16, 128), BF16),
+            vmem((SLOTS, PER * COLS), BF16),
             vmem((3, SLOTS, COLS), F32),
             vmem((NTP, SLOTS, 128), BF16),
             vmem((2, SLOTS, COLS), F32),
@@ -831,10 +841,10 @@
             dma((NTP,)),
             dma((NZ,)),
             dma((NZ,)),
-            dma((2, NEP)),
-            dma((2, NEP)),
-            dma((2, NEP)),
-            dma((2, NEP)),
+            dma((MESSAGES, NEP)),
+            dma((MESSAGES, NEP)),
+            dma((MESSAGES, NEP)),
+            dma((MESSAGES, NEP)),
             dma((NZ,)),
             dma((NZ,)),
             dma((NTP,)),

time: 70 us -> 69 us (0.986)
  Pallas kernels: 69.3 us -> 68.3 us
    pallas_call x1, Pallas kernels: 67.8 us -> 66.8 us  [per_device(): pl.pallas_call(body, out_shape=(pltpu.VMEM((ROWS, COLS), BF16), pltpu.VME...]
where the time goes in v6:
time: 69 us
  Pallas kernels  68.3 us (99%)
    pallas_call x1, Pallas kernels, per_device(): pl.pallas_call(body, out_shape=(pltpu.VMEM((ROWS, COLS), BF16), pltpu.VME...  66.8 us
    pallas_call x1, Pallas kernels, per_device(): pl.pallas_call(state_body, out_shape=(jax.ShapeDtypeStruct((ROWS, COLS),...  1.52 us

profile of v6, /device:TPU:1, one launch (start us, length us, event | category | flops | bytes accessed | tf_op | source)
XLA Modules:
  0.0 69.0 jit_solution(276268913612304481)
XLA Ops:
  0.6 66.8 %shard_map.176 = (bf16[40,256]{1,0:T(8,128)(2,1)S(1)}, f32[40,1,128,128]{3,2,1,0:T(8,128)S(1)}) custom-call(bf16[40,256]{1,0:T(8,128)(2,1)} %hidden.1, s32[1,40]{1,0:T(1,128)} %bitcast.10, f32[40,1,128,128]{3,2,1,0:T(8,128)} %ret_state.1, bf16[256,128]{1,0:T(8,128)(2,1)} %query_weight.1, bf16[256,128]{1,0:T(8,128)(2,1)} %key_weight.1, ...), custom_call_target="tpu_custom_call" | custom-call | tf_op jit(solution)/shard_map/pallas_call | solution.py:787
  67.4 1.5 %shard_map.177 = (bf16[40,256]{1,0:T(8,128)(2,1)}, f32[40,1,128,128]{3,2,1,0:T(8,128)}) custom-call(bf16[40,256]{1,0:T(8,128)(2,1)S(1)} %get-tuple-element.4.before, f32[40,1,128,128]{3,2,1,0:T(8,128)S(1)} %get-tuple-element.5.state), custom_call_target="tpu_custom_call" | custom-call | tf_op jit(solution)/shard_map/pallas_call | solution.py:876
